TPU v7x, 256 devices: a whole 4x4x8 slice. The times are simulated.
256 devices in a mesh: sp: 16 (over y, x), tp: 16 (over z, core).
Axes of the slice: x: 4, y: 4, z: 8, core: 2. Of those that a mesh axis runs over, the one named last changes fastest.
Arguments:
- query_rows: bfloat16 [65536, 1024], P('sp', 'tp'), may hold values from -6 to 6
- key_rows: bfloat16 [65536, 1024], P('sp', 'tp'), may hold values from -6 to 6
- value_rows: bfloat16 [65536, 1024], P('sp', 'tp'), may hold values from -6 to 6
- gate_rows: bfloat16 [65536, 1024], P('sp', 'tp'), may hold values from -6 to 6
- log_decay: float32 [16, 65536], P('tp', 'sp'), may hold values from -1 to 0
- residual: bfloat16 [65536, 2048], P(('sp', 'tp')), may hold values from -6 to 6
- head_gain: float32 [1024], P('tp'), may hold values from 0.1 to 1.9
- out_weight: bfloat16 [1024, 2048], P(None, 'tp'), may hold values from -0.1875 to 0.1875
- norm_gain: float32 [2048], replicated, may hold values from 0.1 to 1.9
- expert_ids: int32 [65536, 2], P(('sp', 'tp')), may hold values from 0 to 15, all different within a row; in each aligned block of 256 rows (0 to 255, 256 to 511, ...) at most 48 rows name the same one
- route_weights: float32 [65536, 2], P(('sp', 'tp')), may hold values from 0.2 to 1
- expert_gate: bfloat16 [2048, 16384], P(None, ('sp', 'tp')), may hold values from -0.125 to 0.125
- expert_up: bfloat16 [2048, 16384], P(None, ('sp', 'tp')), may hold values from -0.125 to 0.125
- expert_down: bfloat16 [2048, 16384], P(None, ('sp', 'tp')), may hold values from -0.1875 to 0.1875
- shared_gate: bfloat16 [2048, 512], replicated, may hold values from -0.125 to 0.125
- shared_up: bfloat16 [2048, 512], replicated, may hold values from -0.125 to 0.125
- shared_down: bfloat16 [2048, 512], replicated, may hold values from -0.25 to 0.25
Outputs:
- result: bfloat16 [65536, 2048], P(('sp', 'tp'))
Inputs may be any that keep to these rules, and one draw needn't show every extreme that they name: `expert_ids`: each row names 2 different experts. Within the rows of one device (aligned blocks of 256 rows) no expert is named by more than 48 rows, and in some block an expert is named by exactly 48 rows.
All inputs are finite; a program needn't handle non-finite values.
Results may differ from a plain program's by a relative error of at most 0.0075.
Values may be sent and summed in bfloat16 or wider, within the bound.
A program may use at most 128 MiB of HBM per device.

v0:
```python
import jax
import jax.numpy as jnp
from jax import lax
from jax.sharding import PartitionSpec as P

HEAD = 64
SPAN = 512


eps = 1e-05


def sent_to_all(value, axis):
    length = lax.axis_size(axis)
    return lax.all_to_all(
        jnp.broadcast_to(value[None], (length, *value.shape)), axis, 0, 0, tiled=True
    )


def all_in_one(value, axis):
    leaves = jax.tree.leaves(value)
    order = sorted(range(len(leaves)), key=lambda k: -leaves[k].size)
    width = (1, *leaves[order[0]].shape)[-1]
    lines = [
        jnp.pad(leaves[k].reshape(-1), (0, -leaves[k].size % width)).reshape(-1, width)
        for k in order
    ]
    both, at, found = (sent_to_all(jnp.concatenate(lines), axis), 0, {})
    for k, line in zip(order, lines):
        share = both[:, at : at + len(line)].reshape(len(both), -1)
        found[k] = share[:, : leaves[k].size].reshape(-1, *leaves[k].shape)
        at += len(line)
    numbers = iter(range(len(leaves)))
    return jax.tree.map(lambda _: found[next(numbers)], value)


def joined_by_halves(pieces, combine):
    while len(jax.tree.leaves(pieces)[0]) > 1:
        pieces = jax.vmap(combine)(
            *(jax.tree.map(lambda part: part[side::2], pieces) for side in (0, 1))
        )
    return jax.tree.map(lambda part: part[0], pieces)


def carried_in(value, axis, combine, identity):
    length, place = (lax.axis_size(axis), lax.axis_index(axis))
    passed = jnp.arange(length) < place

    def kept(part, zero, own):
        part = jnp.where(
            passed.reshape(-1, *(1 for _ in own.shape)), part, jnp.asarray(zero, own.dtype)
        )
        return part

    pieces = all_in_one(value, axis)
    return joined_by_halves(jax.tree.map(kept, pieces, identity, value), combine)


def side_by_side(arrays, axis, dim, along):
    both = jnp.concatenate(arrays, axis=along)
    filled, at, done = (lax.all_gather(both, axis, axis=dim, tiled=True), 0, [])
    for a in arrays:
        done.append(lax.slice_in_dim(filled, at, at + a.shape[along], axis=along))
        at += a.shape[along]
    return tuple(done)


def block_pass(queries, key_heads, values, log_decay, state):
    rows, heads, width = queries.shape
    count = rows // SPAN
    scale = width ** (-0.5)
    query_blocks = queries.reshape(count, SPAN, heads, width)
    key_blocks = key_heads.reshape(count, SPAN, heads, width)
    value_blocks = values.reshape(count, SPAN, heads, width)
    decay_blocks = log_decay.reshape(heads, count, SPAN).transpose(1, 0, 2)
    offsets = jnp.arange(SPAN, dtype=jnp.int32)
    causal = offsets[:, None] >= offsets[None, :]

    def advance(carry, inputs):
        block_queries, block_keys, block_values, decay_block = inputs
        running = jnp.cumsum(decay_block, axis=1)
        spread = running[:, :, None] - running[:, None, :]
        damping = jnp.exp(jnp.where(causal[None], spread, -jnp.inf))
        attention_scores = jnp.einsum(
            "xru,jru->rxj", block_queries, block_keys, preferred_element_type=jnp.float32
        )
        decay_weighted = (attention_scores * scale * damping).astype(jnp.bfloat16)
        inner_block_term = jnp.einsum(
            "svc,csj->vsj", decay_weighted, block_values, preferred_element_type=jnp.float32
        )
        carried = jnp.einsum(
            "nhd,hde->nhe",
            block_queries.astype(jnp.float32),
            carry,
            precision=lax.Precision.HIGHEST,
        )
        carried = carried * jnp.exp(running).T[:, :, None]
        decay_to_block_end = jnp.exp(running[:, -1:] - running).T[:, :, None] * scale
        state_update = jnp.einsum(
            "jok,jow->okw",
            block_keys.astype(jnp.float32) * decay_to_block_end,
            block_values.astype(jnp.float32),
            precision=lax.Precision.HIGHEST,
        )
        carry = carry * jnp.exp(running[:, -1])[:, None, None] + state_update
        return (carry, inner_block_term + carried)

    final, outputs = lax.scan(
        advance, state, (query_blocks, key_blocks, value_blocks, decay_blocks)
    )
    return (final, outputs.reshape(rows, heads, width))


def combine_states(earlier, later):
    return (earlier[0] * later[0], earlier[1] * later[0][:, None, None] + later[1])


def entering_state(totals, own_state):
    identity = (jnp.ones_like(totals), jnp.zeros_like(own_state))
    return carried_in((totals, own_state), "sp", combine_states, identity)[1]


def on_device(
    query_rows,
    key_rows,
    value_rows,
    gate_rows,
    log_decay,
    residual,
    head_gain,
    out_weight,
    norm_gain,
    expert_ids,
    route_weights,
    expert_gate,
    expert_up,
    expert_down,
    shared_gate,
    shared_up,
    shared_down,
):
    seq_rows, local_width = query_rows.shape
    heads = local_width // HEAD
    out_full, gate_full, up_full, down_full = (
        lax.all_gather(out_weight, "tp", axis=1, tiled=True),
        *side_by_side((expert_gate, expert_up, expert_down), "tp", 1, 0),
    )
    queries = query_rows.reshape(seq_rows, heads, HEAD)
    key_heads = key_rows.reshape(seq_rows, heads, HEAD)
    values = value_rows.reshape(seq_rows, heads, HEAD)
    running = jnp.cumsum(log_decay, axis=1)
    totals = jnp.exp(running[:, -1])
    decay_to_block_end = (jnp.exp(running[:, -1:] - running).T * HEAD ** (-0.5))[:, :, None]
    own_state = jnp.einsum(
        "jok,jow->okw",
        key_heads.astype(jnp.float32) * decay_to_block_end,
        values.astype(jnp.float32),
        precision=lax.Precision.HIGHEST,
    )
    incoming = entering_state(totals, own_state)
    _, retained = block_pass(queries, key_heads, values, log_decay, incoming)
    centered = retained - jnp.mean(retained, axis=2, keepdims=True)
    normed = centered * lax.rsqrt(jnp.mean(centered * centered, axis=2, keepdims=True) + eps)
    ret_rows = (
        normed.reshape(seq_rows, local_width)
        * head_gain
        * jax.nn.silu(gate_rows.astype(jnp.float32))
    ).astype(jnp.bfloat16)
    token_rows = lax.all_to_all(ret_rows, "tp", split_axis=0, concat_axis=1, tiled=True)
    mixer = jnp.dot(token_rows, out_full, preferred_element_type=jnp.float32)
    hidden = (residual.astype(jnp.float32) + mixer).astype(jnp.bfloat16)
    hidden_wide = hidden.astype(jnp.float32)
    normed_rows = (
        hidden_wide
        * lax.rsqrt(jnp.mean(hidden_wide * hidden_wide, axis=1, keepdims=True) + eps)
        * norm_gain
    ).astype(jnp.bfloat16)
    shared_mid = (
        jax.nn.silu(jnp.dot(normed_rows, shared_gate, preferred_element_type=jnp.float32))
        * jnp.dot(normed_rows, shared_up, preferred_element_type=jnp.float32)
    ).astype(jnp.bfloat16)
    shared_out = lax.dot_general(
        shared_mid, shared_down, (((1,), (1,)), ((), ())), preferred_element_type=jnp.float32
    )
    specialist_networks = lax.axis_size("sp")
    token_count, chosen_count = expert_ids.shape
    model_width = normed_rows.shape[1]
    capacity = 3 * token_count * chosen_count // (2 * specialist_networks)
    flat_ids = expert_ids.reshape(-1)
    matches = (
        flat_ids[:, None] == jnp.arange(specialist_networks, dtype=jnp.int32)[None, :]
    ).astype(jnp.int32)
    position = jnp.sum((jnp.cumsum(matches, axis=0) - 1) * matches, axis=1)
    slot = flat_ids * capacity + position
    owner = jnp.arange(token_count * chosen_count, dtype=jnp.int32) // chosen_count
    slot_token = jnp.zeros((specialist_networks * capacity,), jnp.int32).at[slot].set(owner)
    slot_live = jnp.zeros((specialist_networks * capacity,), jnp.bfloat16).at[slot].set(1.0)
    outgoing = (normed_rows[slot_token] * slot_live[:, None]).reshape(
        specialist_networks, capacity, model_width
    )
    arrived = lax.all_to_all(outgoing, "sp", split_axis=0, concat_axis=0, tiled=True)
    flat_rows = arrived.reshape(-1, model_width)
    middle = (
        jax.nn.silu(jnp.dot(flat_rows, gate_full, preferred_element_type=jnp.float32))
        * jnp.dot(flat_rows, up_full, preferred_element_type=jnp.float32)
    ).astype(jnp.bfloat16)
    outcome = lax.dot_general(
        middle, down_full, (((1,), (1,)), ((), ())), preferred_element_type=jnp.float32
    ).astype(jnp.bfloat16)
    processed = outcome.reshape(arrived.shape)
    returned = lax.all_to_all(processed, "sp", split_axis=0, concat_axis=0, tiled=True)
    picked = returned.reshape(specialist_networks * capacity, model_width)[slot].astype(jnp.float32)
    decay_weighted = picked * route_weights.reshape(-1)[:, None]
    routed = jnp.sum(decay_weighted.reshape(token_count, chosen_count, model_width), axis=1)
    return (hidden_wide + routed + shared_out).astype(jnp.bfloat16)


def solution(mesh):
    placed = (
        P("sp", "tp"),
        P("sp", "tp"),
        P("sp", "tp"),
        P("sp", "tp"),
        P("tp", "sp"),
        P(("sp", "tp"), None),
        P("tp"),
        P(None, "tp"),
        P(),
        P(("sp", "tp"), None),
        P(("sp", "tp"), None),
        P(None, ("sp", "tp")),
        P(None, ("sp", "tp")),
        P(None, ("sp", "tp")),
        P(),
        P(),
        P(),
    )
    return jax.shard_map(
        on_device, mesh=mesh, in_specs=placed, out_specs=P(("sp", "tp"), None), check_vma=False
    )
```

profile of v0, /device:TPU:1, one launch (start us, length us, event | category | flops | bytes accessed | tf_op | source)
XLA Modules:
  0.0 287.4 jit_solution(11375161928984603023)
XLA Ops:
  6.6 0.7 all-gather.3.cloned.1.call-update
  7.3 2.0 pad_maximum_fusion
  12.7 0.7 fusion.65
  13.6 0.8 broadcast_in_dim.39
  14.4 7.6 %all-to-all-start = ((f32[16,65,64]{1,2,0:T(8,128)}), f32[16,65,64]{1,2,0:T(8,128)}, u32[]{:S(2)}, u32[]{:S(2)}) async-start(f32[16,65,64]{1,2,0:T(8,128)} %broadcast_in_dim.39), calls=%async_computation | async-start | bytes 1048576 | tf_op jit(solution)/shard_map/all_to_all | solution.py:15
  22.5 1.3 copy.64
  23.8 1.0 copy.51
  25.0 1.0 copy.52
  26.1 1.0 copy.53
  27.1 1.1 reduce-window.26
  28.5 4.0 %all-to-all-done = f32[16,65,64]{1,2,0:T(8,128)} async-done(((f32[16,65,64]{1,2,0:T(8,128)}), f32[16,65,64]{1,2,0:T(8,128)}, u32[]{:S(2)}, u32[]{:S(2)}) %all-to-all-start) | async-done | bytes 266272 | tf_op jit(solution)/shard_map/all_to_all | solution.py:15
  32.5 2.0 slice.131
  34.6 1.2 copy.61
  36.8 1.1 fusion.69
  38.2 0.7 fusion.79
  39.0 56.5 %while.13 = (s32[]{:T(128)}, f32[1,64,64]{2,1,0:T(8,128)S(1)}, f32[8,512,1,64]{1,3,2,0:T(8,128)S(1)}, f32[8,1,512]{2,1,0:T(1,128)S(1)}, bf16[8,512,1,64]{1,3,2,0...) while((s32[]{:T(128)}, f32[1,64,64]{2,1,0:T(8,128)S(1)}, ...), condition=%wide.region_5.6_spmd.clone, body=%wide.region_2.5_spmd.clone.sunk | while | flops 119219216 | bytes 885013 | solution.py:108
  39.7 1.5 fusion.130
  41.2 1.1 fusion.131
  44.9 1.1 fusion.129
  46.8 1.5 fusion.130
  48.3 1.1 fusion.131
  52.0 1.1 fusion.129
  53.9 1.5 fusion.130
  55.3 1.1 fusion.131
  59.0 1.1 fusion.129
  60.9 1.5 fusion.130
  62.4 1.1 fusion.131
  63.5 0.6 slice.177
  66.1 1.1 fusion.129
  67.9 1.4 fusion.130
  69.4 1.1 fusion.131
  70.6 0.6 slice.177
  73.1 1.1 fusion.129
  75.0 1.5 fusion.130
  76.5 1.1 fusion.131
  77.7 0.6 slice.177
  80.2 1.1 fusion.129
  82.1 1.5 fusion.130
  83.5 1.1 fusion.131
  87.3 1.1 fusion.129
  89.1 1.5 fusion.130
  90.6 1.1 fusion.131
  94.3 1.1 fusion.129
  97.0 0.8 copy.73
  97.9 10.5 %all-to-all-start.1 = ((bf16[16,256,64]{1,2,0:T(8,128)(2,1)}), bf16[16,256,64]{1,2,0:T(8,128)(2,1)S(1)}, u32[]{:S(2)}, u32[]{:S(2)}) async-start(bf16[16,256,64]{1,2,0:T(8,128)(2,1)} %bitcast.155), calls=%async_computation.1 | async-start | bytes 1048576 | tf_op jit(solution)/shard_map/all_to_all | solution.py:169
  108.8 2.4 scatter_custom_fusion
  111.3 3.9 %scatter_custom_fusion.1 = bf16[768]{0:T(1024)(128)(2,1)S(1)} fusion(s32[512]{0:T(512)S(1)} %bitcast.220, bf16[512]{0:T(512)(128)(2,1)S(1)} %broadcast.246, bf16[]{:T(256)} %constant.89.clone.1), kind=kCustom, calls=%fused_computation.132 | custom fusion | bytes 1538 | tf_op jit(solution)/shard_map/scatter | solution.py:197
  115.3 15.4 %all-to-all-done.1 = bf16[16,256,64]{1,2,0:T(8,128)(2,1)S(1)} async-done(((bf16[16,256,64]{1,2,0:T(8,128)(2,1)}), bf16[16,256,64]{1,2,0:T(8,128)(2,1)S(1)}, u32[]{:S(2)}, u32[]{:S(2)}) %all-to-all-start.1) | async-done | bytes 524320 | tf_op jit(solution)/shard_map/all_to_all | solution.py:169
  130.7 4.0 %fusion.55 = (f32[256]{0:T(256)S(1)}, bf16[256,2048]{1,0:T(8,128)(2,1)S(1)}) fusion(bf16[256,1024]{0,1:T(8,128)(2,1)S(1)} %bitcast.207, bf16[1024,2048]{1,0:T(8,128)(2,1)} %all-gather.3.cloned.1.call-done, bf16[256,2048]{1,0:T(8,128)(2,1)} %param.24), kind=kOutput, calls=%fused_computation.67 | convolution fusion | flops 1076887296 | bytes 6816768 | tf_op jit(solution)/shard_map/dot_general | solution.py:170
  134.8 1.0 copy-done.2
  136.0 4.3 %gather_fusion = bf16[768,2048]{1,0:T(8,128)(2,1)} fusion(bf16[256,2048]{1,0:T(8,128)(2,1)S(1)} %fusion.57, s32[1024]{0:T(1024)S(1)} %pad_clamp_fusion.1), kind=kCustom, calls=%fused_computation | custom fusion | bytes 6294528 | tf_op jit(solution)/shard_map/gather | solution.py:198
  140.4 2.2 broadcast_multiply_fusion
  142.5 42.9 %all_to_all.34 = bf16[16,48,2048]{2,1,0:T(8,128)(2,1)} all-to-all(bf16[16,48,2048]{2,1,0:T(8,128)(2,1)S(1)} %broadcast_multiply_fusion), channel_id=1, replica_groups=mesh['sp'=16,'tp'=16] {'sp'}, dimensions={0} | all-to-all | bytes 6291456 | tf_op jit(solution)/shard_map/all_to_all | solution.py:201
  185.5 6.4 %fusion.46 = f32[768,1024]{1,0:T(8,128)S(1)} fusion(bf16[768,2048]{1,0:T(8,128)(2,1)} %bitcast.198, bf16[6144,1024]{0,1:T(8,128)(2,1)} %all-gather.5.cloned.1.call-done), kind=kOutput, calls=%fused_computation.53 | convolution fusion | flops 3221225472 | bytes 10485760 | tf_op jit(solution)/shard_map/dot_general | solution.py:205
  191.8 1.3 copy-done.15
  193.2 3.9 %multiply_convert_fusion = bf16[768,1024]{1,0:T(8,128)(2,1)S(1)} fusion(f32[768,1024]{1,0:T(8,128)S(1)} %fusion.46, bf16[768,2048]{1,0:T(8,128)(2,1)S(1)} %bitcast.199, bf16[6144,1024]{0,1:T(8,128)(2,1)S(1)} %copy-done.15), kind=kOutput, calls=%fused_computation.59 | convolution fusion | flops 3225944064 | bytes 12058624 | tf_op jit(solution)/shard_map/dot_general | solution.py:204
  197.0 4.9 %fusion.50 = bf16[768,2048]{1,0:T(8,128)(2,1)} fusion(bf16[768,1024]{1,0:T(8,128)(2,1)S(1)} %multiply_convert_fusion, bf16[6144,1024]{0,1:T(8,128)(2,1)S(1)} %copy-done.15), kind=kOutput, calls=%fused_computation.58 | convolution fusion | flops 3222798336 | bytes 8912896 | tf_op jit(solution)/shard_map/dot_general | solution.py:207
  201.9 4.8 %all-to-all-start.3 = ((bf16[16,48,2048]{2,1,0:T(8,128)(2,1)}), bf16[16,48,2048]{2,1,0:T(8,128)(2,1)}, u32[]{:S(2)}, u32[]{:S(2)}) async-start(bf16[16,48,2048]{2,1,0:T(8,128)(2,1)} %bitcast.197), calls=%async_computation.3 | async-start | bytes 6291456 | tf_op jit(solution)/shard_map/all_to_all | solution.py:211
  206.9 3.2 %fusion.99 = f32[256,512]{1,0:T(8,128)} fusion(bf16[2048,512]{1,0:T(8,128)(2,1)} %param.33, bf16[256,2048]{1,0:T(8,128)(2,1)S(1)} %copy-done.3, f32[2048]{0:T(1024)S(1)} %copy-done.11, f32[256]{0:T(256)S(1)} %add_rsqrt_fusion), kind=kOutput, calls=%fused_computation.145 | convolution fusion | flops 538968064 | bytes 3679232 | tf_op jit(solution)/shard_map/dot_general | solution.py:179
  210.1 42.6 %all-to-all-done.3 = bf16[16,48,2048]{2,1,0:T(8,128)(2,1)} async-done(((bf16[16,48,2048]{2,1,0:T(8,128)(2,1)}), bf16[16,48,2048]{2,1,0:T(8,128)(2,1)}, u32[]{:S(2)}, u32[]{:S(2)}) %all-to-all-start.3) | async-done | bytes 3145760 | tf_op jit(solution)/shard_map/all_to_all | solution.py:211
  252.7 7.6 %gather_fusion.1 = bf16[512,2048]{1,0:T(8,128)(2,1)} fusion(bf16[768,2048]{1,0:T(8,128)(2,1)} %bitcast.22, s32[1024]{0:T(1024)S(1)} %pad_clamp_fusion), kind=kCustom, calls=%fused_computation.1 | custom fusion | bytes 4196352 | tf_op jit(solution)/shard_map/gather | solution.py:212
  260.2 5.4 %reshape.495 = f32[256,2,2048]{2,1,0:T(2,128)} reshape(bf16[512,2048]{1,0:T(8,128)(2,1)} %gather_fusion.1) | data formatting | bytes 6291456 | tf_op jit(solution)/shard_map/convert_element_type | solution.py:212
  265.7 10.1 %multiply_reduce_fusion = f32[256,2048]{1,0:T(8,128)} fusion(f32[256,2,2048]{2,1,0:T(2,128)} %reshape.495, f32[256,2]{1,0:T(8,128)S(1)} %copy.60), kind=kLoop, calls=%fused_computation.57 | loop fusion | flops 1572864 | bytes 6293504 | tf_op jit(solution)/shard_map/reduce_sum | solution.py:214
  275.8 4.8 %fusion.53 = bf16[256,2048]{1,0:T(8,128)(2,1)} fusion(bf16[2048,512]{1,0:T(8,128)(2,1)S(1)} %copy-done, f32[256,2048]{1,0:T(8,128)} %multiply_reduce_fusion, bf16[256,2048]{1,0:T(8,128)(2,1)S(1)} %copy-done.3, bf16[2048,512]{1,0:T(8,128)(2,1)} %param.34, f32[256,512]{1,0:T(8,128)} %fusion.99, f32[2048]{0:T(1024)S(1)} %copy-done.11, f32[256]{0:T(256)S(1)} %add_rsqrt_fusion), kind=kOutput, calls=%fused_computation.65 | convolution fusion | flops 1078722560 | bytes 8922112 | tf_op jit(solution)/shard_map/dot_general | solution.py:182
  (172 shorter events, 21.4 us)
Async XLA Ops:
  6.5 269.3 %copy-start = (bf16[2048,512]{1,0:T(8,128)(2,1)S(1)}, bf16[2048,512]{1,0:T(8,128)(2,1)}, u32[]{:S(2)}) copy-start(bf16[2048,512]{1,0:T(8,128)(2,1)} %param.35) | copy-start | bytes 6291460
  6.5 2.9 copy-start.9
  6.5 6.2 %copy-start.5 = (bf16[4096,64]{0,1:T(8,128)(2,1)S(1)}, bf16[4096,64]{0,1:T(8,128)(2,1)}, u32[]{:S(2)}) copy-start(bf16[4096,64]{0,1:T(8,128)(2,1)} %param.20) | copy-start | bytes 1572868
  6.5 6.2 %copy-start.6 = (bf16[4096,64]{0,1:T(8,128)(2,1)S(1)}, bf16[4096,64]{0,1:T(8,128)(2,1)}, u32[]{:S(2)}) copy-start(bf16[4096,64]{0,1:T(8,128)(2,1)} %param.21) | copy-start | bytes 1572868
  6.5 124.2 %all-gather.3.cloned.1.call-start = ((), (), s32[]{:S(2)}) async-start(), calls=%async_computation.4 | async-start | bytes 4456448 | tf_op jit(solution)/shard_map/all_gather | solution.py:145
  7.3 178.2 %all-gather.5.cloned.1.call-start = ((), (), s32[]{:S(2)}) async-start(), calls=%async_computation.5 | async-start | bytes 13369344 | tf_op jit(solution)/shard_map/all_gather | solution.py:61
  9.4 12.7 %copy-start.12 = (s32[256,2]{0,1:T(2,128)S(1)}, s32[256,2]{0,1:T(2,128)}, u32[]{:S(2)}) copy-start(s32[256,2]{0,1:T(2,128)} %param.28) | copy-start | bytes 6148
  14.4 18.1 %all-to-all-start = ((f32[16,65,64]{1,2,0:T(8,128)}), f32[16,65,64]{1,2,0:T(8,128)}, u32[]{:S(2)}, u32[]{:S(2)}) async-start(f32[16,65,64]{1,2,0:T(8,128)} %broadcast_in_dim.39), calls=%async_computation | async-start | bytes 1048576 | tf_op jit(solution)/shard_map/all_to_all | solution.py:15
  22.5 2.3 copy-start.7
  22.5 3.4 %copy-start.8 = (bf16[4096,64]{0,1:T(8,128)(2,1)S(1)}, bf16[4096,64]{0,1:T(8,128)(2,1)}, u32[]{:S(2)}) copy-start(bf16[4096,64]{0,1:T(8,128)(2,1)} %param.19) | copy-start | bytes 1572868
  28.5 10.4 %copy-start.10 = (s32[16,5]{0,1:T(8,128)}, s32[16,5]{0,1:T(8,128)S(1)}, u32[]{:S(2)}) copy-start(s32[16,5]{0,1:T(8,128)S(1)} %reduce-window.27) | copy-start | bytes 964
  95.4 0.7 copy-start.14
  95.6 1.0 copy-start.4
  96.6 12.1 %slice-start = ((s32[16,5]{0,1:T(8,128)}), s32[16,4]{0,1:T(4,128)S(1)}, s32[]{:S(2)}) async-start(s32[16,5]{0,1:T(8,128)} %copy-done.10), calls=%async_computation.6 | async-start | bytes 4096 | tf_op jit(solution)/shard_map/slice.5
  97.9 32.8 %all-to-all-start.1 = ((bf16[16,256,64]{1,2,0:T(8,128)(2,1)}), bf16[16,256,64]{1,2,0:T(8,128)(2,1)S(1)}, u32[]{:S(2)}, u32[]{:S(2)}) async-start(bf16[16,256,64]{1,2,0:T(8,128)(2,1)} %bitcast.155), calls=%async_computation.1 | async-start | bytes 1048576 | tf_op jit(solution)/shard_map/all_to_all | solution.py:169
  130.7 5.0 %copy-start.11 = (f32[2048]{0:T(1024)S(1)}, f32[2048]{0:T(1024)}, u32[]{:S(2)}) copy-start(f32[2048]{0:T(1024)} %param.27) | copy-start | bytes 24580
  134.8 1.0 copy-start.2
  185.5 6.4 %copy-start.1 = (bf16[16,48,2048]{2,1,0:T(8,128)(2,1)S(1)}, bf16[16,48,2048]{2,1,0:T(8,128)(2,1)}, u32[]{:S(2)}) copy-start(bf16[16,48,2048]{2,1,0:T(8,128)(2,1)} %all_to_all.34) | copy-start | bytes 9437188
  185.5 7.7 %copy-start.15 = (bf16[6144,1024]{0,1:T(8,128)(2,1)S(1)}, bf16[6144,1024]{0,1:T(8,128)(2,1)}, u32[]{:S(2)}) copy-start(bf16[6144,1024]{0,1:T(8,128)(2,1)} %all-gather.5.cloned.1.call-done) | copy-start | bytes 37748740
  201.9 4.8 %copy-start.13 = (f32[256,2]{0,1:T(2,128)S(1)}, f32[256,2]{0,1:T(2,128)}, u32[]{:S(2)}) copy-start(f32[256,2]{0,1:T(2,128)} %param.29) | copy-start | bytes 6148
  201.9 5.0 %copy-start.3 = (bf16[256,2048]{1,0:T(8,128)(2,1)S(1)}, bf16[256,2048]{1,0:T(8,128)(2,1)}, u32[]{:S(2)}) copy-start(bf16[256,2048]{1,0:T(8,128)(2,1)} %copy-done.2) | copy-start | bytes 3145732
  201.9 50.8 %all-to-all-start.3 = ((bf16[16,48,2048]{2,1,0:T(8,128)(2,1)}), bf16[16,48,2048]{2,1,0:T(8,128)(2,1)}, u32[]{:S(2)}, u32[]{:S(2)}) async-start(bf16[16,48,2048]{2,1,0:T(8,128)(2,1)} %bitcast.197), calls=%async_computation.3 | async-start | bytes 6291456 | tf_op jit(solution)/shard_map/all_to_all | solution.py:211
Sparse Core Ops, SparseCore 0:
  9.1 53.0 all-gather.2
  64.0 85.5 all-gather.4
where the time goes:
time: 290 us; the launch traced here: 287 us
  waiting for transfers between devices  62.7 us (22%)
  matrix products  57.1 us (20%)
  local copies, waits for them, and re-layouts  51.3 us (18%)
  blocking collectives  42.9 us (15%)
  other arithmetic  24.2 us (8%)
  starting transfers between devices  23.1 us (8%)
  between operations  15.1 us (5%)
  loops' own time  11 us (4%)
    all_to_all x1, blocking collectives, on_device(): lax.all_to_all(outgoing, 'sp', split_axis=0, concat_axis=0, tiled=True)  42.9 us
    all_to_all x1, waiting for transfers between devices, on_device(): lax.all_to_all(processed, 'sp', split_axis=0, concat_axis=0, tiled=True)  42.6 us
    all_to_all x1, waiting for transfers between devices, on_device(): lax.all_to_all(ret_rows, 'tp', split_axis=0, concat_axis=1, tiled=True)  15.4 us
    dot_general x8, matrix products, advance(): jnp.einsum('svc,csj->vsj', decay_weighted, block_values, preferred_elemen...  11.7 us
    another operation x1, loops' own time, block_pass(): lax.scan(advance, state, (query_blocks, key_blocks, value_blocks, decay_b...  11 us
    all_to_all x1, starting transfers between devices, on_device(): lax.all_to_all(ret_rows, 'tp', split_axis=0, concat_axis=1, tiled=True)  10.5 us
    reduce_sum x1, other arithmetic, on_device(): jnp.sum(decay_weighted.reshape(token_count, chosen_count, model_width), a...  10.1 us
    slice x16, local copies, waits for them, and re-layouts, advance(): carry = carry * jnp.exp(running[:, -1])[:, None, None] + state_update  9.42 us
  transfers between devices with their start and end apart: 5, of which 3 were waited for; matrix products, arithmetic and copies ran while one was open for 30% of the time, Pallas kernels for 0%

commit v1 on v0

v1 whole, which is shorter than its diff:
```python
import jax
import jax.numpy as jnp
from jax import lax
from jax.experimental import pallas as pl
from jax.experimental.pallas import tpu as pltpu
from jax.sharding import PartitionSpec as P

HEAD = 64
BLK = 256
EPS = 1e-05
MESH = pl.DeviceIdType.MESH
F32 = jnp.float32
BF16 = jnp.bfloat16
DEPTH = 3

FAR = [(2, 2), (1, 2), (2, 1), (2, 3), (3, 2), (1, 1), (3, 3), (1, 3), (3, 1), (2, 0), (0, 2), (1, 0), (0, 1), (3, 0), (0, 3)]


def dot(a, b, dims=((1,), (0,))):
    return lax.dot_general(a, b, (dims, ((), ())), preferred_element_type=F32)


def halves(x):
    high = x.astype(BF16)
    return high, (x - high.astype(F32)).astype(BF16)


def layer(
    q_h, k_h, v_h, g_h, ld_ref, res_h, hg_ref, ow_h, ng_ref, ids_ref, rw_ref,
    gate_h, up_h, down_h, sg_h, su_h, sd_h,
    out_ref,
    q, k, v, g, res, gst, ust, dst, sg, su, sd,
    owb, gub, dtb, cs, cb, cl, lp, inn, st, sr, pb, rb, tr, hid, nb,
    xs, xr, yb, yr, mid, acc, wt, smid,
    lsem, ssend, srecv, tsend, trecv, rsend, rrecv, dsend, drecv, xsend, xrecv, ysend, yrecv,
):
    sp, tp = lax.axis_index("sp"), lax.axis_index("tp")
    y, x = sp // 4, sp % 4
    z, c = tp // 2, tp % 2
    sibling = z * 2 + (1 - c)

    def partner(m):
        dy, dx = m
        dy, dx = jnp.where(c == 0, dy, dx), jnp.where(c == 0, dx, dy)
        return ((y + dy) % 4) * 4 + (x + dx) % 4

    partners = [partner(m) for m in FAR]

    def local(i, src, to):
        cp = pltpu.make_async_copy(src, to, lsem.at[i])
        cp.start()
        return cp

    c_ow = local(0, ow_h, owb.at[:, pl.ds(pl.multiple_of(tp * 128, 128), 128)])
    c_k = local(1, k_h, k)
    c_v = local(2, v_h, v)
    c_q = local(3, q_h, q)
    c_gate = local(4, gate_h, gst)
    c_up = local(5, up_h, ust)
    c_down = local(6, down_h, dst)
    c_g = local(7, g_h, g)
    c_res = local(8, res_h, res)
    c_sg = local(9, sg_h, sg)
    c_su = local(10, su_h, su)
    c_sd = local(11, sd_h, sd)

    barrier = pltpu.get_barrier_semaphore()
    for other in partners:
        pl.semaphore_signal(barrier, inc=1, device_id=(other, tp), device_id_type=MESH)
    for step in range(1, 16):
        pl.semaphore_signal(barrier, inc=1, device_id=(sp, (tp + step) % 16), device_id_type=MESH)
    pl.semaphore_wait(barrier, 30)

    def piece(p, j):
        if p < 2:
            return owb.at[pl.ds(512 * p, 512), pl.ds(pl.multiple_of(j * 128, 128), 128)]
        if p < 6:
            return gub.at[j // 2, pl.ds(512 * (p - 2), 512), pl.ds(pl.multiple_of((j % 2) * 128, 128), 128)]
        return dtb.at[pl.ds(pl.multiple_of(j * 64 + 32 * (p - 6), 32), 32), :]

    def hop(way, h, p):
        origin = ((z + 8 - h) % 8 if way == 0 else (z + h) % 8) * 2 + c
        to = ((z + 1) % 8 if way == 0 else (z + 7) % 8) * 2 + c
        ref = piece(p, origin)
        return pltpu.make_async_remote_copy(
            ref, ref, rsend.at[way, h, p], rrecv.at[way, h, p], device_id=(sp, to), device_id_type=MESH
        )

    def arrival(way, h, p):
        origin = ((z + 7 - h) % 8 if way == 0 else (z + h + 1) % 8) * 2 + c
        ref = piece(p, origin)
        return pltpu.make_async_remote_copy(
            ref, ref, rsend.at[way, h, p], rrecv.at[way, h, p], device_id=(sp, sibling), device_id_type=MESH
        )

    def across(o, p, core):
        ref = piece(p, ((z + o) % 8) * 2 + core)
        return pltpu.make_async_remote_copy(
            ref, ref, dsend.at[o, p], drecv.at[o, p], device_id=(sp, sibling), device_id_type=MESH
        )

    flying = {0: [], 1: []}
    crossing = []

    def send(way, h, p):
        if len(flying[way]) >= DEPTH:
            flying[way].pop(0).wait_send()
        cp = hop(way, h, p)
        cp.start()
        flying[way].append(cp)

    def cross(o, p):
        cp = across(o, p, c)
        cp.start()
        crossing.append(cp)

    def event(h, p):
        for way in (0, 1):
            last = p % 2 == way
            if h == 0:
                send(way, 0, p)
                continue
            if h == 4 and not last:
                continue
            arrival(way, h - 1, p).wait_recv()
            if h < 3 or (h == 3 and last):
                send(way, h, p)
            cross((8 - h) % 8 if way == 0 else h, p)
        if h == 0:
            cross(0, p)

    order = [(h, p) for h in range(4) for p in (0, 1)]
    order += [(0, 2), (4, 0), (4, 1), (0, 3), (0, 4), (0, 5), (0, 6), (0, 7)]
    order += [(h, p) for h in (1, 2, 3, 4) for p in range(2, 8)]
    events = iter(order)

    def ring(n):
        for _ in range(n):
            at = next(events, None)
            if at is not None:
                event(*at)

    c_ow.wait()
    ring(2)

    ri = lax.broadcasted_iota(jnp.int32, (BLK, BLK), 0)
    ci = lax.broadcasted_iota(jnp.int32, (BLK, BLK), 1)
    upper = (ri <= ci).astype(F32).astype(BF16)
    lower = (ri >= ci).astype(F32).astype(BF16)
    ld = ld_ref[...]
    d0 = ld.astype(BF16)
    left = ld - d0.astype(F32)
    d1 = left.astype(BF16)
    d2 = (left - d1.astype(F32)).astype(BF16)
    cs[...] = dot(d0, upper) + (dot(d1, upper) + dot(d2, upper))
    nt = ((1,), (1,))
    cols = dot(lower, d0, nt) + (dot(lower, d1, nt) + dot(lower, d2, nt))
    for b in range(16):
        cb[b] = jnp.broadcast_to(cols[:, b : b + 1], (BLK, 128))

    c_k.wait()
    c_v.wait()

    def rows(b):
        return pl.ds(pl.multiple_of(b * BLK, BLK), BLK)

    def state_step(b, carry):
        state, total = carry
        cl[b] = state
        lp[b] = jnp.broadcast_to(total, (8, HEAD))
        end = cb[b, BLK - 1 : BLK, :HEAD]
        kd = k[rows(b), :].astype(F32) * (jnp.exp(end - cb[b, :, :HEAD]) * 0.125)
        high, low = halves(kd)
        vb = v[rows(b), :]
        tn = ((0,), (0,))
        state = state * jnp.exp(end) + (dot(high, vb, tn) + dot(low, vb, tn))
        return state, total + end

    state, total = lax.fori_loop(
        0, 16, state_step, (jnp.zeros((HEAD, HEAD), F32), jnp.zeros((1, HEAD), F32))
    )
    st[...] = jnp.concatenate([state, jnp.broadcast_to(total, (HEAD, HEAD))], axis=1)
    scopies = []
    for i, other in enumerate(partners):
        cp = pltpu.make_async_remote_copy(
            st, sr.at[sp], ssend.at[i], srecv.at[i], device_id=(other, tp), device_id_type=MESH
        )
        cp.start()
        scopies.append(cp)
    sr[sp] = st[...]
    ring(1)
    c_q.wait()

    def inner_step(b, _):
        scores = dot(q[rows(b), :], k[rows(b), :], nt)
        wide = jnp.concatenate([cb[b], cb[b]], axis=1)
        spread = wide - cs[pl.ds(b, 1), :]
        damp = jnp.exp(jnp.where(ri >= ci, spread, -jnp.inf))
        inn[b] = dot((scores * 0.125 * damp).astype(BF16), v[rows(b), :])
        return 0

    for part in range(4):
        lax.fori_loop(part * 4, part * 4 + 4, inner_step, 0)
        ring(1)

    c_gate.wait()
    c_up.wait()
    c_down.wait()
    mine = pl.ds(pl.multiple_of(c * 128, 128), 128)

    def pack_step(i, _):
        at = pl.ds(pl.multiple_of(i * 128, 128), 128)
        gub[z, at, mine] = jnp.concatenate([gst[at, :], ust[at, :]], axis=1)
        dtb[pl.ds(pl.multiple_of(tp * 64, 64), 64), at] = dst[at, :].astype(F32).T.astype(BF16)
        return 0

    lax.fori_loop(0, 16, pack_step, 0)
    ring(1)

    for cp in scopies:
        cp.wait_recv()

    def entering(j, inc):
        have = sr[j]
        return jnp.where(j < sp, inc * jnp.exp(have[:, HEAD:]) + have[:, :HEAD], inc)

    inc = lax.fori_loop(0, 16, entering, jnp.zeros((HEAD, HEAD), F32))
    c_g.wait()

    def gated_step(i, _):
        off = (8 + i) % 16
        b = (tp + off) % 16
        high, low = halves(cl[b] + inc * jnp.exp(lp[b, 0:1, :]))
        qb = q[rows(b), :]
        kept = inn[b] + (dot(qb, high) + dot(qb, low)) * jnp.exp(cb[b, :, :HEAD])
        kept = kept - jnp.mean(kept, axis=1, keepdims=True)
        kept = kept * lax.rsqrt(jnp.mean(kept * kept, axis=1, keepdims=True) + EPS)
        rr = kept * hg_ref[...] * jax.nn.silu(g[rows(b), :].astype(F32))
        pb[b] = jnp.concatenate([rr[:128], rr[128:]], axis=1).astype(BF16)

        @pl.when(off != 0)
        def _():
            pltpu.make_async_remote_copy(
                pb.at[b], rb.at[tp], tsend.at[off], trecv.at[off], device_id=(sp, b), device_id_type=MESH
            ).start()

        @pl.when(off == 0)
        def _():
            rb[tp] = pb[b]

        return 0

    for part in range(4):
        lax.fori_loop(part * 4, part * 4 + 4, gated_step, 0)
        ring(PRE[part])

    e_i = lax.broadcasted_iota(jnp.int32, (16, BLK), 0)
    first, second = ids_ref[0:1, :] == e_i, ids_ref[1:2, :] == e_i
    named = jnp.where(first | second, 1.0, 0.0)
    before = dot(named.astype(BF16), (ri < ci).astype(F32).astype(BF16))
    code = jnp.where(named > 0, before, -1.0)
    share = jnp.where(first, rw_ref[0:1, :], 0.0) + jnp.where(second, rw_ref[1:2, :], 0.0)
    codes = jnp.broadcast_to(code[:, None, :], (16, 16, BLK)).reshape(BLK, BLK)
    shares = jnp.broadcast_to(share[:, None, :], (16, 16, BLK)).reshape(BLK, BLK)
    slot = (ri % 16).astype(F32)
    for j in range(3):
        chosen = codes == slot + 16.0 * j
        wt[j] = jnp.where(chosen, 1.0, 0.0).astype(BF16)
        high, low = halves(jnp.where(chosen, shares, 0.0))
        wt[3 + j] = high
        wt[6 + j] = low

    ring(2)

    for off in range(1, 16):
        pltpu.make_async_remote_copy(
            pb.at[0], rb.at[0], tsend.at[off], trecv.at[off], device_id=(sp, sibling), device_id_type=MESH
        ).wait_recv()
    lane = lax.broadcasted_iota(jnp.int32, (128, 128), 1) < 64
    for i in range(8):
        a, b = rb[2 * i].astype(F32), rb[2 * i + 1].astype(F32)
        tr[0:128, 128 * i : 128 * i + 128] = jnp.where(lane, a, pltpu.roll(b, 64, 1)).astype(BF16)
        tr[128:256, 128 * i : 128 * i + 128] = jnp.where(lane, pltpu.roll(a, 64, 1), b).astype(BF16)

    for o in range(8):
        for p in (0, 1):
            across(o, p, 1 - c).wait_recv()
    c_res.wait()

    def wide(n):
        return pl.ds(pl.multiple_of(n * 256, 256), 256)

    def mixer_step(n, squares):
        h = (res[:, wide(n)].astype(F32) + dot(tr[...], owb[:, wide(n)])).astype(BF16)
        hid[:, wide(n)] = h
        h = h.astype(F32)
        h = h * h
        return squares + h[:, :128] + h[:, 128:]

    squares = lax.fori_loop(0, 8, mixer_step, jnp.zeros((BLK, 128), F32))
    scale = lax.rsqrt(jnp.sum(squares, axis=1, keepdims=True) * (1.0 / 2048.0) + EPS)

    def norm_step(n, _):
        nb[:, wide(n)] = (hid[:, wide(n)].astype(F32) * scale * ng_ref[:, wide(n)]).astype(BF16)
        return 0

    lax.fori_loop(0, 8, norm_step, 0)

    xcopies = []
    for j in range(3):

        def pick_step(n, _):
            xs[j, :, :, wide(n)] = dot(wt[j], nb[:, wide(n)]).astype(BF16).reshape(16, 16, 256)
            return 0

        lax.fori_loop(0, 8, pick_step, 0)
        for i, other in enumerate(partners):
            cp = pltpu.make_async_remote_copy(
                xs.at[j, other], xr.at[j, sp], xsend.at[j, i], xrecv.at[j, i], device_id=(other, tp), device_id_type=MESH
            )
            cp.start()
            xcopies.append(cp)
        xr[j, sp] = xs[j, sp]
        ring(1)

    c_sg.wait()
    c_su.wait()

    def shared_step(n, _):
        a = dot(nb[...], sg[:, wide(n)])
        smid[:, wide(n)] = (jax.nn.silu(a) * dot(nb[...], su[:, wide(n)])).astype(BF16)
        return 0

    lax.fori_loop(0, 2, shared_step, 0)
    ring(1)
    c_sd.wait()

    def shared_out(n, _):
        acc[:, wide(n)] = dot(smid[...], sd[wide(n), :], nt) + hid[:, wide(n)].astype(F32)
        return 0

    lax.fori_loop(0, 8, shared_out, 0)
    ring(100)
    for o in range(8):
        for p in range(2, 8):
            across(o, p, 1 - c).wait_recv()

    lane = lax.broadcasted_iota(jnp.int32, (BLK, 128), 1) < 64
    ycopies = []
    for j in range(3):
        for i in range(15):
            xcopies[j * 15 + i].wait_recv()

        def up_step(n, _):
            h = dot(xr[j].reshape(BLK, 2048), gub[n])
            a, b = h[:, :128], h[:, 128:]
            opened = jnp.where(lane, a, pltpu.roll(b, 64, 1))
            lifted = jnp.where(lane, pltpu.roll(a, 64, 1), b)
            mid[:, pl.ds(pl.multiple_of(n * 128, 128), 128)] = (jax.nn.silu(opened) * lifted).astype(BF16)
            return 0

        lax.fori_loop(0, 8, up_step, 0)

        def down_step(n, _):
            yb[j, :, :, wide(n)] = dot(mid[...], dtb[:, wide(n)]).astype(BF16).reshape(16, 16, 256)
            return 0

        lax.fori_loop(0, 8, down_step, 0)
        for i, other in enumerate(partners):
            cp = pltpu.make_async_remote_copy(
                yb.at[j, other], yr.at[j, sp], ysend.at[j, i], yrecv.at[j, i], device_id=(other, tp), device_id_type=MESH
            )
            cp.start()
            ycopies.append(cp)
        yr[j, sp] = yb[j, sp]

    tn = ((0,), (0,))
    for j in range(3):
        for i in range(15):
            ycopies[j * 15 + i].wait_recv()

        def sum_step(n, _):
            back = yr[j, :, :, wide(n)].reshape(BLK, 256)
            sums = acc[:, wide(n)] + (dot(wt[3 + j], back, tn) + dot(wt[6 + j], back, tn))
            if j < 2:
                acc[:, wide(n)] = sums
            else:
                out_ref[:, wide(n)] = sums.astype(BF16)
            return 0

        lax.fori_loop(0, 8, sum_step, 0)

    for cp in scopies + xcopies + ycopies + crossing + flying[0] + flying[1]:
        cp.wait_send()
    for off in range(1, 16):
        pltpu.make_async_remote_copy(
            pb.at[0], rb.at[0], tsend.at[off], trecv.at[off], device_id=(sp, sibling), device_id_type=MESH
        ).wait_send()


PRE = (1, 0, 0, 0)


def on_device(
    query_rows, key_rows, value_rows, gate_rows, log_decay, residual, head_gain, out_weight, norm_gain,
    expert_ids, route_weights, expert_gate, expert_up, expert_down, shared_gate, shared_up, shared_down,
):
    anywhere = pl.BlockSpec(memory_space=pl.ANY)
    inside = pl.BlockSpec(memory_space=pltpu.VMEM)
    dma = pltpu.SemaphoreType.DMA
    vm = pltpu.VMEM
    return pl.pallas_call(
        layer,
        name="layer",
        out_shape=jax.ShapeDtypeStruct((256, 2048), BF16),
        in_specs=[anywhere] * 4 + [inside, anywhere, inside, anywhere, inside, inside, inside] + [anywhere] * 6,
        out_specs=inside,
        scratch_shapes=[
            *[vm((4096, 64), BF16)] * 4,
            vm((256, 2048), BF16),
            *[vm((2048, 64), BF16)] * 3,
            *[vm((2048, 512), BF16)] * 3,
            vm((1024, 2048), BF16),
            vm((8, 2048, 256), BF16),
            vm((1024, 2048), BF16),
            vm((16, 256), F32),
            vm((16, 256, 128), F32),
            vm((16, 64, 64), F32),
            vm((16, 8, 64), F32),
            vm((16, 256, 64), F32),
            vm((64, 128), F32),
            vm((16, 64, 128), F32),
            vm((16, 128, 128), BF16),
            vm((16, 128, 128), BF16),
            vm((256, 1024), BF16),
            vm((256, 2048), BF16),
            vm((256, 2048), BF16),
            *[vm((3, 16, 16, 2048), BF16)] * 4,
            vm((256, 1024), BF16),
            vm((256, 2048), F32),
            vm((9, 256, 256), BF16),
            vm((256, 512), BF16),
            dma((12,)),
            dma((15,)), dma((15,)),
            dma((16,)), dma((16,)),
            dma((2, 4, 8)), dma((2, 4, 8)),
            dma((8, 8)), dma((8, 8)),
            dma((3, 15)), dma((3, 15)),
            dma((3, 15)), dma((3, 15)),
        ],
        compiler_params=pltpu.CompilerParams(
            collective_id=0, has_side_effects=True, vmem_limit_bytes=63 * 1024 * 1024
        ),
    )(
        query_rows, key_rows, value_rows, gate_rows, log_decay.reshape(16, 256), residual,
        head_gain.reshape(1, 64), out_weight, norm_gain.reshape(1, 2048), expert_ids.T, route_weights.T,
        expert_gate, expert_up, expert_down, shared_gate, shared_up, shared_down,
    )


def solution(mesh):
    placed = (
        P("sp", "tp"),
        P("sp", "tp"),
        P("sp", "tp"),
        P("sp", "tp"),
        P("tp", "sp"),
        P(("sp", "tp"), None),
        P("tp"),
        P(None, "tp"),
        P(),
        P(("sp", "tp"), None),
        P(("sp", "tp"), None),
        P(None, ("sp", "tp")),
        P(None, ("sp", "tp")),
        P(None, ("sp", "tp")),
        P(),
        P(),
        P(),
    )
    return jax.shard_map(
        on_device, mesh=mesh, in_specs=placed, out_specs=P(("sp", "tp"), None), check_vma=False
    )
```

time: 290 us -> 183 us (0.63)
  Pallas kernels: 0 us -> 166 us
  waiting for transfers between devices: 62.7 us -> 0 us
  matrix products: 57.1 us -> 0 us
  blocking collectives: 42.9 us -> 0 us
  local copies, waits for them, and re-layouts: 51.3 us -> 14.7 us
  starting transfers between devices: 23.1 us -> 0 us
  other arithmetic: 24.2 us -> 1.4 us
  between operations: 15.1 us -> 0.02 us
  loops' own time: 11 us -> 0 us
    pallas_call x0 -> x1, Pallas kernels: none -> 166 us  [on_device(): pl.pallas_call(layer, name='layer', out_shape=jax.ShapeDtypeStruct((256,...]
    all_to_all x3 -> x0, waiting for transfers between devices: 62 us -> none  [the longest x1 42.6 us: on_device(): lax.all_to_all(processed, 'sp', split_axis=0, concat_axis=0, tiled=True)]
    dot_general x31 -> x0, matrix products: 57.1 us -> none  [the longest x8 11.7 us: advance(): jnp.einsum('svc,csj->vsj', decay_weighted, block_values, preferred_elemen...]
    all_to_all x1 -> x0, blocking collectives: 42.9 us -> none  [on_device(): lax.all_to_all(outgoing, 'sp', split_axis=0, concat_axis=0, tiled=True)]
    all_to_all x3 -> x0, starting transfers between devices: 23 us -> none  [the longest x1 10.5 us: on_device(): lax.all_to_all(ret_rows, 'tp', split_axis=0, concat_axis=1, tiled=True)]
    slice x34 -> x0, local copies, waits for them, and re-layouts: 14.7 us -> none  [the longest x16 9.42 us: advance(): carry = carry * jnp.exp(running[:, -1])[:, None, None] + state_update]
    gather x2 -> x0, local copies, waits for them, and re-layouts: 11.9 us -> none  [the longest x1 7.56 us: on_device(): returned.reshape(specialist_networks * capacity, model_width)[slot]]
    another operation x1 -> x0, loops' own time: 11 us -> none  [block_pass(): lax.scan(advance, state, (query_blocks, key_blocks, value_blocks, decay_b...]
  transfers between devices with their start and end apart: 5 -> 0, of which waited for: 3 -> 0; matrix products, arithmetic and copies ran while one was open for 30% -> 0% of each run, Pallas kernels for 0% -> 0%
where the time goes in v1:
time: 183 us; the launch traced here: 182 us
  Pallas kernels  166 us (91%)
  local copies, waits for them, and re-layouts  14.7 us (8%)
    pallas_call x1, Pallas kernels, on_device(): pl.pallas_call(layer, name='layer', out_shape=jax.ShapeDtypeStruct((256,...  166 us
    unnamed x17, local copies, waits for them, and re-layouts  14.1 us

profile of v1, /device:TPU:1, one launch (start us, length us, event | category | flops | bytes accessed | tf_op | source)
XLA Modules:
  0.0 182.3 jit_solution(7921158004874235907)
XLA Ops:
  0.0 0.0 copy-start.1
  0.0 0.0 copy-start
  0.0 0.5 broadcast.3
  0.5 1.4 reduce.3
  1.9 0.6 reshape.9.ld_ref
  2.5 2.0 %copy.22.gate_h = bf16[2048,64]{1,0:T(8,128)(2,1)} copy(bf16[2048,64]{0,1:T(8,128)(2,1)} %param.28) | data formatting | bytes 524288 | tf_op args[11]
  4.5 2.0 %copy.23.up_h = bf16[2048,64]{1,0:T(8,128)(2,1)} copy(bf16[2048,64]{0,1:T(8,128)(2,1)} %param.29) | data formatting | bytes 524288 | tf_op args[12]
  6.4 0.0 copy-start.2
  6.4 2.0 %copy.24.down_h = bf16[2048,64]{1,0:T(8,128)(2,1)} copy(bf16[2048,64]{0,1:T(8,128)(2,1)} %param.30) | data formatting | bytes 524288 | tf_op args[13]
  8.5 0.0 copy-done
  8.5 0.0 copy-start.3
  8.5 1.3 copy.18.q_h
  9.8 0.0 copy-done.1
  9.8 1.3 copy.19.k_h
  11.1 0.0 copy-done.2
  11.1 1.4 copy.20.v_h
  12.5 0.0 copy-done.3
  12.5 1.3 copy.21.g_h
  13.8 166.1 %layer.1 = bf16[256,2048]{1,0:T(8,128)(2,1)} custom-call(bf16[4096,64]{1,0:T(8,128)(2,1)} %copy.18.q_h, bf16[4096,64]{1,0:T(8,128)(2,1)} %copy.19.k_h, bf16[4096,64]{1,0:T(8,128)(2,1)} %copy.20.v_h, bf16[4096,64]{1,0:T(8,128)(2,1)} %copy.21.g_h, f32[16,256]{1,0:T(8,128)} %reshape.9.ld_ref, bf16[256,2048]{1,0:T(8,128)(2,1)} %res_h.1, f32[1,64]{1,0:T(1,128)} %bitcast.7, ...), custom_call_target="tpu_custom_call" | custom-call | tf_op jit(solution)/shard_map/layer/pallas_call | solution.py:412
  180.0 2.3 %copy.26 = bf16[256,2048]{1,0:T(8,128)(2,1)} copy(bf16[256,2048]{1,0:T(8,128)(2,1)} %layer.1) | data formatting | bytes 2097152
Async XLA Ops:
  0.0 9.8 %copy-start.1 = (bf16[4096,64]{0,1:T(8,128)(2,1)S(1)}, bf16[4096,64]{0,1:T(8,128)(2,1)}, u32[]{:S(2)}) copy-start(bf16[4096,64]{0,1:T(8,128)(2,1)} %param.18) | copy-start | bytes 1572868
  0.0 8.5 %copy-start = (bf16[4096,64]{0,1:T(8,128)(2,1)S(1)}, bf16[4096,64]{0,1:T(8,128)(2,1)}, u32[]{:S(2)}) copy-start(bf16[4096,64]{0,1:T(8,128)(2,1)} %param.17) | copy-start | bytes 1572868
  6.4 4.7 %copy-start.2 = (bf16[4096,64]{0,1:T(8,128)(2,1)S(1)}, bf16[4096,64]{0,1:T(8,128)(2,1)}, u32[]{:S(2)}) copy-start(bf16[4096,64]{0,1:T(8,128)(2,1)} %param.19) | copy-start | bytes 1572868
  8.5 4.0 %copy-start.3 = (bf16[4096,64]{0,1:T(8,128)(2,1)S(1)}, bf16[4096,64]{0,1:T(8,128)(2,1)}, u32[]{:S(2)}) copy-start(bf16[4096,64]{0,1:T(8,128)(2,1)} %param.20) | copy-start | bytes 1572868

commit v2 on v1

v2 whole, which is shorter than its diff:
```python
import jax
import jax.numpy as jnp
from jax import lax
from jax.experimental import pallas as pl
from jax.experimental.pallas import tpu as pltpu
from jax.sharding import PartitionSpec as P

HEAD = 64
BLK = 256
EPS = 1e-05
MESH = pl.DeviceIdType.MESH
F32 = jnp.float32
BF16 = jnp.bfloat16
DEPTH = 3

FAR = [(2, 2), (1, 2), (2, 1), (2, 3), (3, 2), (1, 1), (3, 3), (1, 3), (3, 1), (2, 0), (0, 2), (1, 0), (0, 1), (3, 0), (0, 3)]


def dot(a, b, dims=((1,), (0,))):
    return lax.dot_general(a, b, (dims, ((), ())), preferred_element_type=F32)


def halves(x):
    high = x.astype(BF16)
    return high, (x - high.astype(F32)).astype(BF16)


def layer(
    q_h, k_h, v_h, g_h, ld_ref, res_h, hg_ref, ow_h, ng_ref, ids_ref, rw_ref,
    gate_h, up_h, down_h, sg_h, su_h, sd_h,
    out_ref,
    q, k, v, g, res, sg, su, sd, ows, owb, gateb, upb, downb,
    cs, cb, cl, lp, inn, st, sr, pb, rb, tr, hid, nb,
    xs, xr, yb, yr, mid, acc, wt, smid,
    lsem, ssend, srecv, tsend, trecv, osend, orecv, wsend, wrecv, vsend, vrecv,
    rsend, rrecv, dsend, drecv, xsend, xrecv, ysend, yrecv,
):
    sp, tp = lax.axis_index("sp"), lax.axis_index("tp")
    y, x = sp // 4, sp % 4
    z, c = tp // 2, tp % 2
    sibling = z * 2 + (1 - c)
    nt, tn = ((1,), (1,)), ((0,), (0,))

    def partner(m):
        dy, dx = m
        dy, dx = jnp.where(c == 0, dy, dx), jnp.where(c == 0, dx, dy)
        return ((y + dy) % 4) * 4 + (x + dx) % 4

    partners = [partner(m) for m in FAR]

    def remote(src, to, here, there, device):
        return pltpu.make_async_remote_copy(src, to, here, there, device_id=device, device_id_type=MESH)

    def local(i, src, to):
        cp = pltpu.make_async_copy(src, to, lsem.at[i])
        cp.start()
        return cp

    def block(ref, size, i):
        return ref.at[pl.ds(pl.multiple_of(i * size, size), size)]

    c_ow = local(0, ow_h, ows)
    c_gate = local(1, gate_h, block(gateb, 64, tp))
    c_up = local(2, up_h, block(upb, 64, tp))
    c_down = local(3, down_h, block(downb, 64, tp))
    c_k = local(4, k_h, k)
    c_v = local(5, v_h, v)
    c_q = local(6, q_h, q)
    c_g = local(7, g_h, g)
    c_res = local(8, res_h, res)
    c_sg = local(9, sg_h, sg)
    c_su = local(10, su_h, su)
    c_sd = local(11, sd_h, sd)

    barrier = pltpu.get_barrier_semaphore()
    for other in partners:
        pl.semaphore_signal(barrier, inc=1, device_id=(other, tp), device_id_type=MESH)
    for step in range(1, 16):
        pl.semaphore_signal(barrier, inc=1, device_id=(sp, (tp + step) % 16), device_id_type=MESH)
    pl.semaphore_wait(barrier, 30)

    def piece(p, j):
        ref = (gateb, upb, downb)[p // 2]
        return ref.at[pl.ds(pl.multiple_of(j * 64 + 32 * (p % 2), 32), 32)]

    def hop(way, h, p):
        origin = ((z + 8 - h) % 8 if way == 0 else (z + h) % 8) * 2 + c
        to = ((z + 1) % 8 if way == 0 else (z + 7) % 8) * 2 + c
        ref = piece(p, origin)
        return remote(ref, ref, rsend.at[way, h, p], rrecv.at[way, h, p], (sp, to))

    def arrival(way, h, p):
        origin = ((z + 7 - h) % 8 if way == 0 else (z + h + 1) % 8) * 2 + c
        ref = piece(p, origin)
        return remote(ref, ref, rsend.at[way, h, p], rrecv.at[way, h, p], (sp, sibling))

    def across(o, p, core):
        ref = piece(p, ((z + o) % 8) * 2 + core)
        return remote(ref, ref, dsend.at[o, p], drecv.at[o, p], (sp, sibling))

    flying = {0: [], 1: []}
    started = []

    def go(cp):
        cp.start()
        started.append(cp)
        return cp

    def send(way, h, p):
        if len(flying[way]) >= DEPTH:
            flying[way].pop(0).wait_send()
        cp = hop(way, h, p)
        cp.start()
        flying[way].append(cp)

    def event(h, p):
        for way in (0, 1):
            last = p % 2 == way
            if h == 0:
                send(way, 0, p)
                continue
            if h == 4 and not last:
                continue
            arrival(way, h - 1, p).wait_recv()
            if h < 3 or (h == 3 and last):
                send(way, h, p)
            go(across((8 - h) % 8 if way == 0 else h, p, c))
        if h == 0:
            go(across(0, p, c))

    events = [(h, p) for h in range(5) for p in range(6)]

    def ring(n):
        for _ in range(n):
            if events:
                event(*events.pop(0))

    def slice_of(core):
        return pl.ds(pl.multiple_of(sp * 64 + core * 32, 32), 32)

    def columns_of(j):
        return pl.ds(pl.multiple_of(j * 128, 128), 128)

    c_ow.wait()
    for step in range(1, 16):
        other = (tp + step) % 16
        go(remote(
            ows.at[slice_of((c + step) % 2), :], owb.at[slice_of((c + step) % 2), columns_of(tp)],
            osend.at[step], orecv.at[step], (sp, other),
        ))
    owb[slice_of(c), columns_of(tp)] = ows[slice_of(c), :]
    c_gate.wait()
    c_up.wait()
    c_down.wait()
    ring(FIRST)

    ri = lax.broadcasted_iota(jnp.int32, (BLK, BLK), 0)
    ci = lax.broadcasted_iota(jnp.int32, (BLK, BLK), 1)
    upper = (ri <= ci).astype(F32).astype(BF16)
    lower = (ri >= ci).astype(F32).astype(BF16)
    for b in range(16):
        cs[b : b + 1, :] = ld_ref[0:1, b * BLK : b * BLK + BLK]
    ld = cs[...]
    d0 = ld.astype(BF16)
    left = ld - d0.astype(F32)
    d1 = left.astype(BF16)
    d2 = (left - d1.astype(F32)).astype(BF16)
    cs[...] = dot(d0, upper) + (dot(d1, upper) + dot(d2, upper))
    cols = dot(lower, d0, nt) + (dot(lower, d1, nt) + dot(lower, d2, nt))
    for b in range(16):
        cb[b] = jnp.broadcast_to(cols[:, b : b + 1], (BLK, 128))

    c_k.wait()
    c_v.wait()

    def at(b):
        return pl.ds(pl.multiple_of(b * BLK, BLK), BLK)

    def state_step(b, carry):
        state, total = carry
        cl[b] = state
        lp[b] = jnp.broadcast_to(total, (8, 128))
        end = cb[b, BLK - 1 : BLK, :]
        wide = jnp.concatenate([end, end], axis=1)
        kd = k[:, at(b)].astype(F32) * (jnp.exp(wide - cs[pl.ds(b, 1), :]) * 0.125)
        high, low = halves(kd)
        vb = v[:, at(b)]
        state = state * jnp.exp(end[:, :HEAD]) + (dot(vb, high, nt) + dot(vb, low, nt))
        return state, total + end

    state, total = lax.fori_loop(
        0, 16, state_step, (jnp.zeros((HEAD, HEAD), F32), jnp.zeros((1, 128), F32)), unroll=2
    )
    st[0:32] = jnp.concatenate([state[:32], state[32:]], axis=1)
    st[32:40] = jnp.broadcast_to(total, (8, 128))
    scopies = []
    for i, other in enumerate(partners):
        scopies.append(go(remote(st, sr.at[sp], ssend.at[i], srecv.at[i], (other, tp))))
    sr[sp] = st[...]

    for step in range(1, 16):
        remote(
            ows.at[slice_of(c), :], owb.at[slice_of(c), columns_of(tp)], osend.at[step], orecv.at[step], (sp, sibling)
        ).wait_recv()

    def rows_of(s, core):
        return owb.at[pl.ds(pl.multiple_of(s * 64 + core * 32, 32), 32)]

    wcopies = []
    for i, other in enumerate(partners):
        wcopies.append(go(remote(rows_of(sp, c), rows_of(sp, c), wsend.at[i], wrecv.at[i], (other, tp))))
    go(remote(rows_of(sp, c), rows_of(sp, c), vsend.at[15], vrecv.at[15], (sp, sibling)))
    ring(1)
    c_q.wait()

    def inner_step(b, _):
        scores = dot(k[:, at(b)], q[:, at(b)], tn)
        spread = cs[pl.ds(b, 1), :] - jnp.concatenate([cb[b], cb[b]], axis=1)
        damp = jnp.exp(jnp.where(ri <= ci, spread, -jnp.inf))
        inn[b] = dot(v[:, at(b)], (scores * 0.125 * damp).astype(BF16))
        return 0

    for part in range(2):
        lax.fori_loop(part * 8, part * 8 + 8, inner_step, 0, unroll=2)
        ring(1)

    e_i = lax.broadcasted_iota(jnp.int32, (16, BLK), 0)
    first, second = ids_ref[0:1, :] == e_i, ids_ref[1:2, :] == e_i
    named = jnp.where(first | second, 1.0, 0.0)
    before = dot(named.astype(BF16), (ri < ci).astype(F32).astype(BF16))
    code = jnp.where(named > 0, before, -1.0)
    share = jnp.where(first, rw_ref[0:1, :], 0.0) + jnp.where(second, rw_ref[1:2, :], 0.0)
    codes = jnp.broadcast_to(code[:, None, :], (16, 16, BLK)).reshape(BLK, BLK)
    shares = jnp.broadcast_to(share[:, None, :], (16, 16, BLK)).reshape(BLK, BLK)
    slot = (ri % 16).astype(F32)
    for j in range(3):
        chosen = codes == slot + 16.0 * j
        wt[j] = jnp.where(chosen, 1.0, 0.0).astype(BF16)
        high, low = halves(jnp.where(chosen, shares, 0.0).T)
        wt[3 + j] = high
        wt[6 + j] = low

    gain = jnp.broadcast_to(hg_ref[...], (BLK, HEAD)).T
    c_g.wait()
    for cp in scopies:
        cp.wait_recv()

    def entering(j, inc):
        have = sr[j]
        return jnp.where(j < sp, inc * jnp.exp(have[32:33]) + have[:32], inc)

    packed = lax.fori_loop(0, 16, entering, jnp.zeros((32, 128), F32))
    inc = jnp.concatenate([packed[:, :HEAD], packed[:, HEAD:]], axis=0)

    def gated(i):
        off = (8 + i) % 16
        b = (tp + off) % 16
        high, low = halves(cl[b] + inc * jnp.exp(lp[b, 0:1, :HEAD]))
        qb = q[:, at(b)]
        kept = inn[b] + (dot(high, qb) + dot(low, qb)) * jnp.exp(cs[pl.ds(b, 1), :])
        kept = kept - jnp.mean(kept, axis=0, keepdims=True)
        kept = kept * lax.rsqrt(jnp.mean(kept * kept, axis=0, keepdims=True) + EPS)
        pb[b] = (kept * gain * jax.nn.silu(g[:, at(b)].astype(F32))).astype(BF16)
        return off, b

    def gated_step(i, _):
        pairs = [gated(2 * i), gated(2 * i + 1)]
        for off, b in pairs:

            @pl.when(off != 0)
            def _():
                remote(pb.at[b], rb.at[tp], tsend.at[off], trecv.at[off], (sp, b)).start()

            @pl.when(off == 0)
            def _():
                rb[tp] = pb[b]

        return 0

    lax.fori_loop(0, 8, gated_step, 0)
    ring(AFTER_GATED)

    for i, other in enumerate(partners):
        dy, dx = FAR[i]
        origin = partner(((4 - dy) % 4, (4 - dx) % 4))
        wcopies[i].wait_recv()
        go(remote(rows_of(origin, c), rows_of(origin, c), vsend.at[i], vrecv.at[i], (sp, sibling)))

    for off in range(1, 16):
        remote(pb.at[0], rb.at[0], tsend.at[off], trecv.at[off], (sp, sibling)).wait_recv()
    for i in range(8):
        both = jnp.concatenate([rb[2 * i], rb[2 * i + 1]], axis=0)
        tr[:, 128 * i : 128 * i + 128] = both.astype(F32).T.astype(BF16)
    ring(1)
    for i in range(16):
        remote(rows_of(sp, c), rows_of(sp, c), vsend.at[i], vrecv.at[i], (sp, sibling)).wait_recv()
    c_res.wait()

    def wide(n):
        return pl.ds(pl.multiple_of(n * 256, 256), 256)

    def mixer_step(n, squares):
        h = (res[:, wide(n)].astype(F32) + dot(tr[...], owb[:, wide(n)])).astype(BF16)
        hid[:, wide(n)] = h
        h = h.astype(F32)
        h = h * h
        return squares + h[:, :128] + h[:, 128:]

    squares = lax.fori_loop(0, 8, mixer_step, jnp.zeros((BLK, 128), F32))
    scale = lax.rsqrt(jnp.sum(squares, axis=1, keepdims=True) * (1.0 / 2048.0) + EPS)
    ring(1)

    def norm_step(n, _):
        nb[:, wide(n)] = (hid[:, wide(n)].astype(F32) * scale * ng_ref[:, wide(n)]).astype(BF16)
        return 0

    lax.fori_loop(0, 8, norm_step, 0)

    xcopies = []
    for j in range(3):

        def pick_step(n, _):
            xs[j, :, :, wide(n)] = dot(wt[j], nb[:, wide(n)]).astype(BF16).reshape(16, 16, 256)
            return 0

        lax.fori_loop(0, 8, pick_step, 0)
        for i, other in enumerate(partners):
            xcopies.append(go(remote(xs.at[j, other], xr.at[j, sp], xsend.at[j, i], xrecv.at[j, i], (other, tp))))
        xr[j, sp] = xs[j, sp]
        ring(1)

    c_sg.wait()
    c_su.wait()

    def shared_step(n, _):
        a = dot(nb[...], sg[:, wide(n)])
        smid[:, wide(n)] = (jax.nn.silu(a) * dot(nb[...], su[:, wide(n)])).astype(BF16)
        return 0

    lax.fori_loop(0, 2, shared_step, 0)
    ring(1)
    c_sd.wait()

    def shared_out(n, _):
        acc[:, wide(n)] = dot(smid[...], sd[wide(n), :], nt) + hid[:, wide(n)].astype(F32)
        return 0

    lax.fori_loop(0, 8, shared_out, 0)
    ring(len(events) - 12)

    def opened(j, n):
        at_n = pl.ds(pl.multiple_of(n * 128, 128), 128)
        rows = xr[j].reshape(BLK, 2048)
        h = dot(rows, jnp.concatenate([gateb[at_n, :], upb[at_n, :]], axis=0), nt)
        mid[:, at_n] = (jax.nn.silu(h[:, :128]) * h[:, 128:]).astype(BF16)

    def landed(offsets, pieces):
        for o in offsets:
            for p in pieces:
                across(o, p, 1 - c).wait_recv()

    for i in range(15):
        xcopies[i].wait_recv()

    def near(i, _):
        opened(0, (z + i + 6) % 8)
        return 0

    def third(i, _):
        opened(0, (z + 3 + 2 * i) % 8)
        return 0

    landed((0, 1, 2, 6, 7), range(4))
    lax.fori_loop(0, 5, near, 0)
    ring(6)
    landed((3, 5), range(4))
    lax.fori_loop(0, 2, third, 0)
    ring(4)
    landed((4,), range(4))
    opened(0, (z + 4) % 8)
    ring(2)
    landed(range(8), (4, 5))

    ycopies = []
    for j in range(3):
        if j > 0:
            for i in range(15):
                xcopies[j * 15 + i].wait_recv()

            def up_step(n, _):
                opened(j, n)
                return 0

            lax.fori_loop(0, 8, up_step, 0)

        def down_step(n, _):
            yb[j, :, :, wide(n)] = dot(mid[...], downb[:, wide(n)]).astype(BF16).reshape(16, 16, 256)
            return 0

        lax.fori_loop(0, 8, down_step, 0)
        for i, other in enumerate(partners):
            ycopies.append(go(remote(yb.at[j, other], yr.at[j, sp], ysend.at[j, i], yrecv.at[j, i], (other, tp))))
        yr[j, sp] = yb[j, sp]

    for j in range(3):
        for i in range(15):
            ycopies[j * 15 + i].wait_recv()

        def sum_step(n, _):
            back = yr[j, :, :, wide(n)].reshape(BLK, 256)
            sums = acc[:, wide(n)] + (dot(wt[3 + j], back) + dot(wt[6 + j], back))
            if j < 2:
                acc[:, wide(n)] = sums
            else:
                out_ref[:, wide(n)] = sums.astype(BF16)
            return 0

        lax.fori_loop(0, 8, sum_step, 0)

    for cp in started + flying[0] + flying[1]:
        cp.wait_send()
    for off in range(1, 16):
        remote(pb.at[0], rb.at[0], tsend.at[off], trecv.at[off], (sp, sibling)).wait_send()


FIRST = 3
AFTER_GATED = 2


def on_device(
    query_rows, key_rows, value_rows, gate_rows, log_decay, residual, head_gain, out_weight, norm_gain,
    expert_ids, route_weights, expert_gate, expert_up, expert_down, shared_gate, shared_up, shared_down,
):
    anywhere = pl.BlockSpec(memory_space=pl.ANY)
    inside = pl.BlockSpec(memory_space=pltpu.VMEM)
    dma = pltpu.SemaphoreType.DMA
    vm = pltpu.VMEM
    return pl.pallas_call(
        layer,
        name="layer",
        out_shape=jax.ShapeDtypeStruct((256, 2048), BF16),
        in_specs=[anywhere] * 4 + [inside, anywhere, inside, anywhere, inside, inside, inside] + [anywhere] * 6,
        out_specs=inside,
        scratch_shapes=[
            *[vm((64, 4096), BF16)] * 4,
            vm((256, 2048), BF16),
            *[vm((2048, 512), BF16)] * 3,
            vm((1024, 128), BF16),
            *[vm((1024, 2048), BF16)] * 4,
            vm((16, 256), F32),
            vm((16, 256, 128), F32),
            vm((16, 64, 64), F32),
            vm((16, 8, 128), F32),
            vm((16, 64, 256), F32),
            vm((40, 128), F32),
            vm((16, 40, 128), F32),
            vm((16, 64, 256), BF16),
            vm((16, 64, 256), BF16),
            vm((256, 1024), BF16),
            vm((256, 2048), BF16),
            vm((256, 2048), BF16),
            *[vm((3, 16, 16, 2048), BF16)] * 4,
            vm((256, 1024), BF16),
            vm((256, 2048), F32),
            vm((9, 256, 256), BF16),
            vm((256, 512), BF16),
            dma((12,)),
            dma((15,)), dma((15,)),
            dma((16,)), dma((16,)),
            dma((16,)), dma((16,)),
            dma((15,)), dma((15,)),
            dma((16,)), dma((16,)),
            dma((2, 4, 6)), dma((2, 4, 6)),
            dma((8, 6)), dma((8, 6)),
            dma((3, 15)), dma((3, 15)),
            dma((3, 15)), dma((3, 15)),
        ],
        compiler_params=pltpu.CompilerParams(
            collective_id=0, has_side_effects=True, vmem_limit_bytes=63 * 1024 * 1024
        ),
    )(
        query_rows.T, key_rows.T, value_rows.T, gate_rows.T, log_decay, residual,
        head_gain.reshape(1, 64), out_weight, norm_gain.reshape(1, 2048), expert_ids.T, route_weights.T,
        expert_gate.T, expert_up.T, expert_down.T, shared_gate, shared_up, shared_down,
    )


def solution(mesh):
    placed = (
        P("sp", "tp"),
        P("sp", "tp"),
        P("sp", "tp"),
        P("sp", "tp"),
        P("tp", "sp"),
        P(("sp", "tp"), None),
        P("tp"),
        P(None, "tp"),
        P(),
        P(("sp", "tp"), None),
        P(("sp", "tp"), None),
        P(None, ("sp", "tp")),
        P(None, ("sp", "tp")),
        P(None, ("sp", "tp")),
        P(),
        P(),
        P(),
    )
    return jax.shard_map(
        on_device, mesh=mesh, in_specs=placed, out_specs=P(("sp", "tp"), None), check_vma=False
    )
```

time: 183 us -> 143 us (0.78)
  Pallas kernels: 166 us -> 140 us
  local copies, waits for them, and re-layouts: 14.7 us -> 2.3 us
    pallas_call x1, Pallas kernels: 166 us -> 140 us  [on_device(): pl.pallas_call(layer, name='layer', out_shape=jax.ShapeDtypeStruct((256,...]
    unnamed x17 -> x1, local copies, waits for them, and re-layouts: 14.1 us -> 2.3 us
where the time goes in v2:
time: 143 us
  Pallas kernels  140 us (98%)
  local copies, waits for them, and re-layouts  2.3 us (2%)
    pallas_call x1, Pallas kernels, on_device(): pl.pallas_call(layer, name='layer', out_shape=jax.ShapeDtypeStruct((256,...  140 us

profile of v2, /device:TPU:1, one launch (start us, length us, event | category | flops | bytes accessed | tf_op | source)
XLA Modules:
  0.0 142.8 jit_solution(13633459027574181087)
XLA Ops:
  0.0 140.5 %layer.1 = bf16[256,2048]{1,0:T(8,128)(2,1)} custom-call(bf16[64,4096]{1,0:T(8,128)(2,1)} %bitcast.11, bf16[64,4096]{1,0:T(8,128)(2,1)} %bitcast.12, bf16[64,4096]{1,0:T(8,128)(2,1)} %bitcast.13, bf16[64,4096]{1,0:T(8,128)(2,1)} %bitcast.14, f32[1,4096]{1,0:T(1,128)} %ld_ref.1, bf16[256,2048]{1,0:T(8,128)(2,1)} %res_h.1, f32[1,64]{1,0:T(1,128)} %bitcast.21, ...), custom_call_target="tpu_custom_call" | custom-call | tf_op jit(solution)/shard_map/layer/pallas_call | solution.py:438
  140.5 2.3 %copy.19 = bf16[256,2048]{1,0:T(8,128)(2,1)} copy(bf16[256,2048]{1,0:T(8,128)(2,1)} %layer.1) | data formatting | bytes 2097152

commit v3 on v2

--- a/solution.py
+++ b/solution.py
@@ -12,6 +12,7 @@
 F32 = jnp.float32
 BF16 = jnp.bfloat16
 DEPTH = 3
+PARTS = 2
 
 FAR = [(2, 2), (1, 2), (2, 1), (2, 3), (3, 2), (1, 1), (3, 3), (1, 3), (3, 1), (2, 0), (0, 2), (1, 0), (0, 1), (3, 0), (0, 3)]
 
@@ -323,9 +324,13 @@
             xs[j, :, :, wide(n)] = dot(wt[j], nb[:, wide(n)]).astype(BF16).reshape(16, 16, 256)
             return 0
 
-        lax.fori_loop(0, 8, pick_step, 0)
-        for i, other in enumerate(partners):
-            xcopies.append(go(remote(xs.at[j, other], xr.at[j, sp], xsend.at[j, i], xrecv.at[j, i], (other, tp))))
+        for part in range(PARTS):
+            lax.fori_loop(part * 8 // PARTS, (part + 1) * 8 // PARTS, pick_step, 0)
+            cols = pl.ds(part * 2048 // PARTS, 2048 // PARTS)
+            for i, other in enumerate(partners):
+                xcopies.append(go(remote(
+                    xs.at[j, other, :, cols], xr.at[j, sp, :, cols], xsend.at[j, part, i], xrecv.at[j, part, i], (other, tp)
+                )))
         xr[j, sp] = xs[j, sp]
         ring(1)
 
@@ -359,7 +364,7 @@
             for p in pieces:
                 across(o, p, 1 - c).wait_recv()
 
-    for i in range(15):
+    for i in range(15 * PARTS):
         xcopies[i].wait_recv()
 
     def near(i, _):
@@ -384,8 +389,8 @@
     ycopies = []
     for j in range(3):
         if j > 0:
-            for i in range(15):
-                xcopies[j * 15 + i].wait_recv()
+            for i in range(15 * PARTS):
+                xcopies[j * 15 * PARTS + i].wait_recv()
 
             def up_step(n, _):
                 opened(j, n)
@@ -397,15 +402,16 @@
             yb[j, :, :, wide(n)] = dot(mid[...], downb[:, wide(n)]).astype(BF16).reshape(16, 16, 256)
             return 0
 
-        lax.fori_loop(0, 8, down_step, 0)
-        for i, other in enumerate(partners):
-            ycopies.append(go(remote(yb.at[j, other], yr.at[j, sp], ysend.at[j, i], yrecv.at[j, i], (other, tp))))
+        for part in range(PARTS):
+            lax.fori_loop(part * 8 // PARTS, (part + 1) * 8 // PARTS, down_step, 0)
+            cols = pl.ds(part * 2048 // PARTS, 2048 // PARTS)
+            for i, other in enumerate(partners):
+                ycopies.append(go(remote(
+                    yb.at[j, other, :, cols], yr.at[j, sp, :, cols], ysend.at[j, part, i], yrecv.at[j, part, i], (other, tp)
+                )))
         yr[j, sp] = yb[j, sp]
 
     for j in range(3):
-        for i in range(15):
-            ycopies[j * 15 + i].wait_recv()
-
         def sum_step(n, _):
             back = yr[j, :, :, wide(n)].reshape(BLK, 256)
             sums = acc[:, wide(n)] + (dot(wt[3 + j], back) + dot(wt[6 + j], back))
@@ -415,7 +421,10 @@
                 out_ref[:, wide(n)] = sums.astype(BF16)
             return 0
 
-        lax.fori_loop(0, 8, sum_step, 0)
+        for part in range(PARTS):
+            for i in range(15):
+                ycopies[(j * PARTS + part) * 15 + i].wait_recv()
+            lax.fori_loop(part * 8 // PARTS, (part + 1) * 8 // PARTS, sum_step, 0)
 
     for cp in started + flying[0] + flying[1]:
         cp.wait_send()
@@ -472,8 +481,8 @@
             dma((16,)), dma((16,)),
             dma((2, 4, 6)), dma((2, 4, 6)),
             dma((8, 6)), dma((8, 6)),
-            dma((3, 15)), dma((3, 15)),
-            dma((3, 15)), dma((3, 15)),
+            dma((3, PARTS, 15)), dma((3, PARTS, 15)),
+            dma((3, PARTS, 15)), dma((3, PARTS, 15)),
         ],
         compiler_params=pltpu.CompilerParams(
             collective_id=0, has_side_effects=True, vmem_limit_bytes=63 * 1024 * 1024

time: 143 us -> 138 us (0.965)
  Pallas kernels: 140 us -> 135 us
    pallas_call x1, Pallas kernels: 140 us -> 135 us  [on_device(): pl.pallas_call(layer, name='layer', out_shape=jax.ShapeDtypeStruct((256,...]
where the time goes in v3:
time: 138 us
  Pallas kernels  135 us (98%)
  local copies, waits for them, and re-layouts  2.3 us (2%)
    pallas_call x1, Pallas kernels, on_device(): pl.pallas_call(layer, name='layer', out_shape=jax.ShapeDtypeStruct((256,...  135 us

profile of v3, /device:TPU:1, one launch (start us, length us, event | category | flops | bytes accessed | tf_op | source)
XLA Modules:
  0.0 137.7 jit_solution(11805954230920376077)
XLA Ops:
  0.0 135.3 %layer.1 = bf16[256,2048]{1,0:T(8,128)(2,1)} custom-call(bf16[64,4096]{1,0:T(8,128)(2,1)} %bitcast.11, bf16[64,4096]{1,0:T(8,128)(2,1)} %bitcast.12, bf16[64,4096]{1,0:T(8,128)(2,1)} %bitcast.13, bf16[64,4096]{1,0:T(8,128)(2,1)} %bitcast.14, f32[1,4096]{1,0:T(1,128)} %ld_ref.1, bf16[256,2048]{1,0:T(8,128)(2,1)} %res_h.1, f32[1,64]{1,0:T(1,128)} %bitcast.21, ...), custom_call_target="tpu_custom_call" | custom-call | tf_op jit(solution)/shard_map/layer/pallas_call | solution.py:447
  135.4 2.3 %copy.19 = bf16[256,2048]{1,0:T(8,128)(2,1)} copy(bf16[256,2048]{1,0:T(8,128)(2,1)} %layer.1) | data formatting | bytes 2097152

commit v4 on v3

--- a/solution.py
+++ b/solution.py
@@ -11,7 +11,7 @@
 MESH = pl.DeviceIdType.MESH
 F32 = jnp.float32
 BF16 = jnp.bfloat16
-DEPTH = 3
+DEPTH = 2
 PARTS = 2
 
 FAR = [(2, 2), (1, 2), (2, 1), (2, 3), (3, 2), (1, 1), (3, 3), (1, 3), (3, 1), (2, 0), (0, 2), (1, 0), (0, 1), (3, 0), (0, 3)]
@@ -81,8 +81,10 @@
     pl.semaphore_wait(barrier, 30)
 
     def piece(p, j):
-        ref = (gateb, upb, downb)[p // 2]
-        return ref.at[pl.ds(pl.multiple_of(j * 64 + 32 * (p % 2), 32), 32)]
+        rows = pl.ds(pl.multiple_of(j * 64 + 32 * (p % 2), 32), 32)
+        if p < 4:
+            return (gateb, upb)[p // 2].at[rows]
+        return downb.at[rows, pl.ds(1024 * (p // 2 - 2), 1024)]
 
     def hop(way, h, p):
         origin = ((z + 8 - h) % 8 if way == 0 else (z + h) % 8) * 2 + c
@@ -100,6 +102,7 @@
         return remote(ref, ref, dsend.at[o, p], drecv.at[o, p], (sp, sibling))
 
     flying = {0: [], 1: []}
+    depth = [DEPTH]
     started = []
 
     def go(cp):
@@ -108,7 +111,7 @@
         return cp
 
     def send(way, h, p):
-        if len(flying[way]) >= DEPTH:
+        if len(flying[way]) >= depth[0]:
             flying[way].pop(0).wait_send()
         cp = hop(way, h, p)
         cp.start()
@@ -129,7 +132,18 @@
         if h == 0:
             go(across(0, p, c))
 
-    events = [(h, p) for h in range(5) for p in range(6)]
+    events = [(h, p) for h in range(3) for p in range(4)]
+    for first, count, more in (
+        (4, 2, [(3, p) for p in range(4)]),
+        (None, 0, [(1, 4), (1, 5), (0, 6), (0, 7)] + [(4, p) for p in range(4)]),
+        (None, 0, [(2, 4), (2, 5), (1, 6), (1, 7), (3, 4), (3, 5), (2, 6), (2, 7)]),
+        (None, 0, [(4, 4), (4, 5), (3, 6), (3, 7), (4, 6), (4, 7)]),
+    ):
+        events += [(0, first + i) for i in range(count)] + more
+    total_events = len(events)
+
+    def ring_to(n):
+        ring(n - (total_events - len(events)))
 
     def ring(n):
         for _ in range(n):
@@ -204,13 +218,25 @@
             ows.at[slice_of(c), :], owb.at[slice_of(c), columns_of(tp)], osend.at[step], orecv.at[step], (sp, sibling)
         ).wait_recv()
 
-    def rows_of(s, core):
-        return owb.at[pl.ds(pl.multiple_of(s * 64 + core * 32, 32), 32)]
-
-    wcopies = []
-    for i, other in enumerate(partners):
-        wcopies.append(go(remote(rows_of(sp, c), rows_of(sp, c), wsend.at[i], wrecv.at[i], (other, tp))))
-    go(remote(rows_of(sp, c), rows_of(sp, c), vsend.at[15], vrecv.at[15], (sp, sibling)))
+    def part_of(s, a):
+        return owb.at[pl.ds(pl.multiple_of(s * 64 + c * 32 + a * 16, 16), 16)]
+
+    def placed(a, along, other):
+        return partner((along % 4, other % 4) if a == 0 else (other % 4, along % 4))
+
+    routes = [(2, 0), (1, 0), (3, 0)]
+    for d, _ in routes:
+        for a in (0, 1):
+            go(remote(part_of(sp, a), part_of(sp, a), wsend.at[a, d, 0], wrecv.at[a, d, 0], (placed(a, d, 0), tp)))
+
+    def pass_on(a, d0):
+        ref = part_of(placed(a, 4 - d0, 0), a) if d0 else part_of(sp, a)
+        for d in (2, 1, 3):
+            go(remote(ref, ref, wsend.at[a, d0, d], wrecv.at[a, d0, d], (placed(a, 0, d), tp)))
+        go(remote(ref, ref, vsend.at[a, d0, 0], vrecv.at[a, d0, 0], (sp, sibling)))
+
+    for a in (0, 1):
+        pass_on(a, 0)
     ring(1)
     c_q.wait()
 
@@ -224,6 +250,11 @@
     for part in range(2):
         lax.fori_loop(part * 8, part * 8 + 8, inner_step, 0, unroll=2)
         ring(1)
+    for d0, _ in routes:
+        for a in (0, 1):
+            ref = part_of(placed(a, 4 - d0, 0), a)
+            remote(ref, ref, wsend.at[a, d0, 0], wrecv.at[a, d0, 0], (sp, sibling)).wait_recv()
+            pass_on(a, d0)
 
     e_i = lax.broadcasted_iota(jnp.int32, (16, BLK), 0)
     first, second = ids_ref[0:1, :] == e_i, ids_ref[1:2, :] == e_i
@@ -281,11 +312,12 @@
     lax.fori_loop(0, 8, gated_step, 0)
     ring(AFTER_GATED)
 
-    for i, other in enumerate(partners):
-        dy, dx = FAR[i]
-        origin = partner(((4 - dy) % 4, (4 - dx) % 4))
-        wcopies[i].wait_recv()
-        go(remote(rows_of(origin, c), rows_of(origin, c), vsend.at[i], vrecv.at[i], (sp, sibling)))
+    for d0 in (0, 2, 1, 3):
+        for a in (0, 1):
+            for d in (2, 1, 3):
+                ref = part_of(placed(a, 4 - d0, 4 - d), a)
+                remote(ref, ref, wsend.at[a, d0, d], wrecv.at[a, d0, d], (sp, sibling)).wait_recv()
+                go(remote(ref, ref, vsend.at[a, d0, d], vrecv.at[a, d0, d], (sp, sibling)))
 
     for off in range(1, 16):
         remote(pb.at[0], rb.at[0], tsend.at[off], trecv.at[off], (sp, sibling)).wait_recv()
@@ -293,8 +325,10 @@
         both = jnp.concatenate([rb[2 * i], rb[2 * i + 1]], axis=0)
         tr[:, 128 * i : 128 * i + 128] = both.astype(F32).T.astype(BF16)
     ring(1)
-    for i in range(16):
-        remote(rows_of(sp, c), rows_of(sp, c), vsend.at[i], vrecv.at[i], (sp, sibling)).wait_recv()
+    for d0 in range(4):
+        for a in (0, 1):
+            for d in range(4):
+                remote(part_of(sp, a), part_of(sp, a), vsend.at[a, d0, d], vrecv.at[a, d0, d], (sp, sibling)).wait_recv()
     c_res.wait()
 
     def wide(n):
@@ -351,21 +385,30 @@
         return 0
 
     lax.fori_loop(0, 8, shared_out, 0)
-    ring(len(events) - 12)
+    depth[0] = 8
+    ring_to(14)
 
     def opened(j, n):
         at_n = pl.ds(pl.multiple_of(n * 128, 128), 128)
         rows = xr[j].reshape(BLK, 2048)
         h = dot(rows, jnp.concatenate([gateb[at_n, :], upb[at_n, :]], axis=0), nt)
-        mid[:, at_n] = (jax.nn.silu(h[:, :128]) * h[:, 128:]).astype(BF16)
+        mid[j, :, at_n] = (jax.nn.silu(h[:, :128]) * h[:, 128:]).astype(BF16)
 
     def landed(offsets, pieces):
         for o in offsets:
             for p in pieces:
                 across(o, p, 1 - c).wait_recv()
 
-    for i in range(15 * PARTS):
-        xcopies[i].wait_recv()
+    def came(j):
+        for i in range(15 * PARTS):
+            xcopies[j * 15 * PARTS + i].wait_recv()
+
+    def opened_some(j, begin, end):
+        def up_step(n, _):
+            opened(j, n)
+            return 0
+
+        lax.fori_loop(begin, end, up_step, 0)
 
     def near(i, _):
         opened(0, (z + i + 6) % 8)
@@ -375,65 +418,75 @@
         opened(0, (z + 3 + 2 * i) % 8)
         return 0
 
+    ycopies = {}
+
+    def closed(j, part):
+        def down_step(n, _):
+            yb[j, :, :, wide(n)] = dot(mid[j], downb[:, wide(n)]).astype(BF16).reshape(16, 16, 256)
+            return 0
+
+        lax.fori_loop(part * 4, part * 4 + 4, down_step, 0)
+        cols = pl.ds(part * 1024, 1024)
+        ycopies[j, part] = [
+            go(remote(
+                yb.at[j, other, :, cols], yr.at[j, sp, :, cols], ysend.at[j, part, i], yrecv.at[j, part, i], (other, tp)
+            ))
+            for i, other in enumerate(partners)
+        ]
+        yr[j, sp, :, cols] = yb[j, sp, :, cols]
+
+    came(0)
     landed((0, 1, 2, 6, 7), range(4))
     lax.fori_loop(0, 5, near, 0)
-    ring(6)
+    ring_to(18)
     landed((3, 5), range(4))
     lax.fori_loop(0, 2, third, 0)
-    ring(4)
+    ring_to(26)
     landed((4,), range(4))
     opened(0, (z + 4) % 8)
-    ring(2)
+    ring_to(30)
+    came(1)
+    for begin, end, events_done in ((0, 3, 32), (3, 6, 34), (6, 8, 36)):
+        opened_some(1, begin, end)
+        ring_to(events_done)
     landed(range(8), (4, 5))
-
-    ycopies = []
+    closed(0, 0)
+    closed(1, 0)
+    ring_to(38)
+    came(2)
+    opened_some(2, 0, 8)
+    closed(2, 0)
+    ring_to(40)
+    landed(range(8), (6, 7))
     for j in range(3):
-        if j > 0:
-            for i in range(15 * PARTS):
-                xcopies[j * 15 * PARTS + i].wait_recv()
-
-            def up_step(n, _):
-                opened(j, n)
+        closed(j, 1)
+
+    for cp in started[: -15 * 6] + flying[0] + flying[1]:
+        cp.wait_send()
+    for part in range(2):
+        for j in range(3):
+
+            def sum_step(n, _):
+                back = yr[j, :, :, wide(n)].reshape(BLK, 256)
+                sums = acc[:, wide(n)] + (dot(wt[3 + j], back) + dot(wt[6 + j], back))
+                if j < 2:
+                    acc[:, wide(n)] = sums
+                else:
+                    out_ref[:, wide(n)] = sums.astype(BF16)
                 return 0
 
-            lax.fori_loop(0, 8, up_step, 0)
-
-        def down_step(n, _):
-            yb[j, :, :, wide(n)] = dot(mid[...], downb[:, wide(n)]).astype(BF16).reshape(16, 16, 256)
-            return 0
-
-        for part in range(PARTS):
-            lax.fori_loop(part * 8 // PARTS, (part + 1) * 8 // PARTS, down_step, 0)
-            cols = pl.ds(part * 2048 // PARTS, 2048 // PARTS)
-            for i, other in enumerate(partners):
-                ycopies.append(go(remote(
-                    yb.at[j, other, :, cols], yr.at[j, sp, :, cols], ysend.at[j, part, i], yrecv.at[j, part, i], (other, tp)
-                )))
-        yr[j, sp] = yb[j, sp]
-
-    for j in range(3):
-        def sum_step(n, _):
-            back = yr[j, :, :, wide(n)].reshape(BLK, 256)
-            sums = acc[:, wide(n)] + (dot(wt[3 + j], back) + dot(wt[6 + j], back))
-            if j < 2:
-                acc[:, wide(n)] = sums
-            else:
-                out_ref[:, wide(n)] = sums.astype(BF16)
-            return 0
-
-        for part in range(PARTS):
-            for i in range(15):
-                ycopies[(j * PARTS + part) * 15 + i].wait_recv()
-            lax.fori_loop(part * 8 // PARTS, (part + 1) * 8 // PARTS, sum_step, 0)
-
-    for cp in started + flying[0] + flying[1]:
+            for cp in ycopies[j, part]:
+                cp.wait_recv()
+            lax.fori_loop(part * 4, part * 4 + 4, sum_step, 0)
+
+    for cp in started[-15 * 6 :]:
         cp.wait_send()
     for off in range(1, 16):
         remote(pb.at[0], rb.at[0], tsend.at[off], trecv.at[off], (sp, sibling)).wait_send()
 
 
-FIRST = 3
-AFTER_GATED = 2
+FIRST = 2
+AFTER_GATED = 1
 
 
 def on_device(
@@ -469,7 +522,7 @@
             vm((256, 2048), BF16),
             vm((256, 2048), BF16),
             *[vm((3, 16, 16, 2048), BF16)] * 4,
-            vm((256, 1024), BF16),
+            vm((3, 256, 1024), BF16),
             vm((256, 2048), F32),
             vm((9, 256, 256), BF16),
             vm((256, 512), BF16),
@@ -477,10 +530,10 @@
             dma((15,)), dma((15,)),
             dma((16,)), dma((16,)),
             dma((16,)), dma((16,)),
-            dma((15,)), dma((15,)),
-            dma((16,)), dma((16,)),
-            dma((2, 4, 6)), dma((2, 4, 6)),
-            dma((8, 6)), dma((8, 6)),
+            dma((2, 4, 4)), dma((2, 4, 4)),
+            dma((2, 4, 4)), dma((2, 4, 4)),
+            dma((2, 4, 8)), dma((2, 4, 8)),
+            dma((8, 8)), dma((8, 8)),
             dma((3, PARTS, 15)), dma((3, PARTS, 15)),
             dma((3, PARTS, 15)), dma((3, PARTS, 15)),
         ],

time: 138 us -> 137 us (level)
  no operation moved by 1% of the time
where the time goes in v4:
time: 137 us; the launch traced here: 136 us
  Pallas kernels  134 us (98%)
  local copies, waits for them, and re-layouts  2.3 us (2%)
    pallas_call x1, Pallas kernels, on_device(): pl.pallas_call(layer, name='layer', out_shape=jax.ShapeDtypeStruct((256,...  134 us

profile of v4, /device:TPU:1, one launch (start us, length us, event | category | flops | bytes accessed | tf_op | source)
XLA Modules:
  0.0 136.5 jit_solution(4659574560879770999)
XLA Ops:
  0.0 134.2 %layer.1 = bf16[256,2048]{1,0:T(8,128)(2,1)} custom-call(bf16[64,4096]{1,0:T(8,128)(2,1)} %bitcast.11, bf16[64,4096]{1,0:T(8,128)(2,1)} %bitcast.12, bf16[64,4096]{1,0:T(8,128)(2,1)} %bitcast.13, bf16[64,4096]{1,0:T(8,128)(2,1)} %bitcast.14, f32[1,4096]{1,0:T(1,128)} %ld_ref.1, bf16[256,2048]{1,0:T(8,128)(2,1)} %res_h.1, f32[1,64]{1,0:T(1,128)} %bitcast.21, ...), custom_call_target="tpu_custom_call" | custom-call | tf_op jit(solution)/shard_map/layer/pallas_call | solution.py:500
  134.2 2.3 %copy.19 = bf16[256,2048]{1,0:T(8,128)(2,1)} copy(bf16[256,2048]{1,0:T(8,128)(2,1)} %layer.1) | data formatting | bytes 2097152
